TPU v7x, 256 devices: a 4x2x16 block of a 4x16x16 slice. The times are simulated.
256 devices in a mesh: grp: 2 (over y), sp: 16 (over z), tp: 8 (over x, core).
Axes of the slice: x: 4, y: 2, z: 16, core: 2. Of those that a mesh axis runs over, the one named last changes fastest.
The devices are a block of a 4x16x16 slice.
Arguments:
- tokens: bfloat16 [65536, 2048], P(('grp', 'sp')), parts along dimension 0, may hold values from -6 to 6
- in_gain: float32 [2048], replicated, may hold values from 0.1 to 1.9
- w_input: bfloat16 [2048, 2048], P(None, 'tp'), may hold values from -0.125 to 0.125
- w_gate: bfloat16 [2048, 2048], P(None, 'tp'), may hold values from -4 to 4
- conv_taps: float32 [4, 2048], P(None, 'tp'), may hold values from -3 to 3
- w_rate: bfloat16 [8, 256, 256], P('tp'), may hold values from -0.375 to 0.375
- w_inlet: bfloat16 [8, 256, 256], P('tp'), may hold values from -0.375 to 0.375
- decay_param: float32 [2048], P('tp'), may hold values from 3 to 25
- decay_bias: float32 [8, 65536], P('tp', ('grp', 'sp')), parts along dimension 1, may hold values from -1.5 to 0
- out_gain: float32 [2048], P('tp'), may hold values from 0.1 to 1.9
- w_out: bfloat16 [2048, 2048], P('sp'), may hold values from -0.125 to 0.125
Outputs:
- mixer_out: bfloat16 [65536, 2048], P(('grp', 'sp', 'tp')), parts along dimension 0
There are 2 independent parts, one for each index of `grp`. A program takes and returns all parts, laid end to end along the dimension named above; an argument that names none is the same for every part. Nothing has to cross between parts.
All inputs are finite; a program needn't handle non-finite values.
Results may differ from a plain program's by a relative error of at most 0.013.
Values may be sent and summed in bfloat16 or wider, within the bound.
A program may use at most 128 MiB of HBM per device.

v0:
```python
import jax
import jax.numpy as jnp
from jax import lax
from jax.sharding import PartitionSpec as P


def from_behind(array, axis, by):
    peers = lax.axis_size(axis)
    pairs = [(i, i + by) for i in range(peers) if 0 <= i + by < peers]
    return lax.ppermute(array, axis, pairs)


def sent_to_all(array, axis):
    copies = jnp.broadcast_to(array, (lax.axis_size(axis), *array.shape))
    return lax.all_to_all(copies, axis, split_axis=0, concat_axis=0, tiled=True)


def collected_together(array, axis):
    leaves = jax.tree.leaves(array)
    sequence = sorted(range(len(leaves)), key=lambda k: -leaves[k].size)
    width = (1, *leaves[sequence[0]].shape)[-1]
    lines = [
        jnp.pad(leaves[k].reshape(-1), (0, -leaves[k].size % width)).reshape(-1, width)
        for k in sequence
    ]
    both, at, found = (sent_to_all(jnp.concatenate(lines), axis), 0, {})
    for k, line in zip(sequence, lines):
        piece = both[:, at : at + len(line)].reshape(len(both), -1)
        found[k] = piece[:, : leaves[k].size].reshape(-1, *leaves[k].shape)
        at += len(line)
    numbers = iter(range(len(leaves)))
    return jax.tree.map(lambda _: found[next(numbers)], array)


def joined_by_halves(pieces, combine):
    while len(jax.tree.leaves(pieces)[0]) > 1:
        pieces = jax.vmap(combine)(
            *(jax.tree.map(lambda part: part[side::2], pieces) for side in (0, 1))
        )
    return jax.tree.map(lambda part: part[0], pieces)


def entering(array, axis, combine, identity):
    peers, position = (lax.axis_size(axis), lax.axis_index(axis))
    passed = jnp.arange(peers) < position

    def kept(part, zero, own):
        part = jnp.where(
            passed.reshape(-1, *(1 for _ in own.shape)), part, jnp.asarray(zero, own.dtype)
        )
        return part

    pieces = collected_together(array, axis)
    return joined_by_halves(jax.tree.map(kept, pieces, identity, array), combine)


def of_everyone(array, axis):
    everything = sent_to_all(array, axis)
    return jnp.sum(everything, axis=0)


def combine_pairs(first_pair, second_pair):
    return (first_pair[0] * second_pair[0], second_pair[0] * first_pair[1] + second_pair[1])


def blocked_scan(decay_factor, drive_term):
    row_count, width = decay_factor.shape
    block_count = row_count // 8
    decay_blocks = decay_factor.reshape(block_count, 8, width)
    drive_blocks = drive_term.reshape(block_count, 8, width)
    running_prod = decay_blocks[:, 0]
    running_state = drive_blocks[:, 0]
    prod_list = [running_prod]
    state_list = [running_state]
    for inner in range(1, 8):
        factor = decay_blocks[:, inner]
        running_prod = factor * running_prod
        running_state = factor * running_state + drive_blocks[:, inner]
        prod_list.append(running_prod)
        state_list.append(running_state)
    prod_inner = jnp.stack(prod_list, axis=1)
    state_inner = jnp.stack(state_list, axis=1)
    total_prod = running_prod
    total_state = running_state
    stride = 1
    while stride < block_count:
        earlier_prod = jnp.concatenate(
            [jnp.ones((stride, width), jnp.float32), total_prod[: block_count - stride]], axis=0
        )
        earlier_state = jnp.concatenate(
            [jnp.zeros((stride, width), jnp.float32), total_state[: block_count - stride]], axis=0
        )
        total_prod, total_state = combine_pairs(
            (earlier_prod, earlier_state), (total_prod, total_state)
        )
        stride = stride * 2
    before_prod = jnp.concatenate(
        [jnp.ones((1, width), jnp.float32), total_prod[: block_count - 1]], axis=0
    )
    before_state = jnp.concatenate(
        [jnp.zeros((1, width), jnp.float32), total_state[: block_count - 1]], axis=0
    )
    full_prod = prod_inner * before_prod[:, None, :]
    full_local = state_inner + prod_inner * before_state[:, None, :]
    return (full_prod.reshape(row_count, width), full_local.reshape(row_count, width))


def body(
    tokens,
    in_gain,
    w_input,
    w_gate,
    conv_taps,
    w_rate,
    w_inlet,
    decay_param,
    decay_bias,
    out_gain,
    w_out,
):
    row_count = tokens.shape[0]
    channels = w_input.shape[1]
    heads_here = w_rate.shape[0]
    head_size = w_rate.shape[1]
    conv_reach = conv_taps.shape[0] - 1
    as_float = tokens.astype(jnp.float32)
    inv_norm = lax.rsqrt(jnp.mean(as_float * as_float, axis=1, keepdims=True) + 1e-06)
    normed = (as_float * inv_norm * in_gain).astype(jnp.bfloat16)
    projected = jnp.dot(normed, w_input, preferred_element_type=jnp.float32).astype(jnp.bfloat16)
    gate_raw = jnp.dot(normed, w_gate, preferred_element_type=jnp.float32).astype(jnp.bfloat16)
    prior_rows = from_behind(projected[row_count - conv_reach :], "sp", 1)
    padded = jnp.concatenate([prior_rows, projected], axis=0).astype(jnp.float32)
    summed = padded[0:row_count] * conv_taps[0]
    for offset in range(1, conv_reach + 1):
        summed = summed + padded[offset : offset + row_count] * conv_taps[offset]
    convolved = summed.astype(jnp.bfloat16)
    per_head = convolved.reshape(row_count, heads_here, head_size)
    rate_gate = jax.nn.sigmoid(
        jnp.einsum("shi,hij->shj", per_head, w_rate, preferred_element_type=jnp.float32)
    ).reshape(row_count, channels)
    input_gate = jax.nn.sigmoid(
        jnp.einsum("shi,hij->shj", per_head, w_inlet, preferred_element_type=jnp.float32)
    ).reshape(row_count, channels)
    head_bias = jnp.repeat(jnp.transpose(decay_bias), head_size, axis=1)
    log_decay = -8.0 * rate_gate * jax.nn.softplus(-decay_param) + head_bias
    decay_factor = jnp.exp(log_decay)
    drive_term = jnp.sqrt(-jnp.expm1(2.0 * log_decay)) * input_gate * convolved.astype(jnp.float32)
    unit_full = (jnp.ones((channels,), jnp.float32), jnp.zeros((channels,), jnp.float32))
    decay_prod, local_state = blocked_scan(decay_factor, drive_term)
    incoming_state = entering((decay_prod[-1], local_state[-1]), "sp", combine_pairs, unit_full)[1]
    full_state = local_state + decay_prod * incoming_state
    gated_out = full_state * jax.nn.gelu(gate_raw.astype(jnp.float32))
    square_total = of_everyone(jnp.sum(gated_out * gated_out, axis=1), "tp")
    out_scale = lax.rsqrt(square_total / (channels * lax.axis_size("tp")) + 1e-06)
    normed_out = (gated_out * out_scale[:, None] * out_gain).astype(jnp.bfloat16)
    token_matrix = lax.all_to_all(normed_out, "tp", split_axis=0, concat_axis=1, tiled=True)
    projected_out = jnp.dot(
        token_matrix,
        lax.all_gather(w_out, "sp", axis=0, tiled=True),
        preferred_element_type=jnp.float32,
    )
    return projected_out.astype(jnp.bfloat16)


def solution(mesh):
    return jax.shard_map(
        body,
        mesh=mesh,
        in_specs=(
            P(("grp", "sp"), None),
            P(),
            P(None, "tp"),
            P(None, "tp"),
            P(None, "tp"),
            P("tp", None, None),
            P("tp", None, None),
            P("tp"),
            P("tp", ("grp", "sp")),
            P("tp"),
            P("sp", None),
        ),
        out_specs=P(("grp", "sp", "tp"), None),
        check_vma=False,
    )
```

profile of v0, /device:TPU:33, one launch (start us, length us, event | category | flops | bytes accessed | tf_op | source)
XLA Modules:
  0.0 142.6 jit_solution(2775839110201704660)
XLA Ops:
  6.6 0.7 all-gather.2.cloned.1.call-update
  7.3 5.2 %fusion = f32[2048]{0:T(1024)S(1)} fusion(bf16[2048,2048]{1,0:T(8,128)(2,1)} %param.11), kind=kLoop, calls=%fused_computation.2 | loop fusion | flops 12580864 | bytes 8396800 | tf_op jit(solution)/shard_map/reduce_sum | solution.py:127
  12.6 0.5 copy-done.2
  13.1 4.0 %convolution_convert_fusion.2 = bf16[2048,256]{1,0:T(8,128)(2,1)S(1)} fusion(bf16[2048,256]{1,0:T(8,128)(2,1)} %param.13, bf16[2048,2048]{1,0:T(8,128)(2,1)S(1)} %copy-done.2, f32[2048]{0:T(1024)S(1)} %copy-done.9, f32[2048]{0:T(1024)S(1)} %add_rsqrt_fusion.1), kind=kOutput, calls=%fused_computation.21 | convolution fusion | flops 2164785152 | bytes 10502144 | tf_op jit(solution)/shard_map/dot_general | solution.py:129
  17.1 5.4 %collective-permute-start = (bf16[3,256]{1,0:T(4,128)(2,1)S(1)}, bf16[3,256]{1,0:T(4,128)(2,1)S(1)}, u32[]{:S(2)}, u32[]{:S(2)}) collective-permute-start(bf16[3,256]{1,0:T(4,128)(2,1)S(1)} %slice.253), channel_id=1, source_target_pairs={{0,8},{8,16},{16,24},{24,32},{32,40},{40,48},{48,56},{56,64},{64,7... | collective-permute-start | bytes 4616 | tf_op jit(solution)/shard_map/ppermute | solution.py:10
  22.6 0.5 broadcast.117
  23.1 0.7 reduce.4
  23.8 0.1 reshape.114
  23.9 0.2 maximum_convert_fusion
  24.2 0.9 fusion.20
  25.1 0.7 fusion.8
  25.9 0.8 fusion.24
  26.7 2.0 %fusion.27 = f32[256,8,256]{2,1,0:T(8,128)S(1)} fusion(bf16[2048,256]{1,0:T(8,128)(2,1)S(1)} %fusion.20, f32[2048,256]{1,0:T(8,128)S(1)} %fusion.8, f32[2048]{0:T(1024)S(1)} %bitcast.74, f32[256]{0:T(256)S(1)} %fusion.34, bf16[1,256,256]{2,1,0:T(8,128)(2,1)S(1)} %copy-done.8), kind=kOutput, calls=%fused_computation.44 | convolution fusion | flops 273678336 | bytes 5383168 | tf_op jit(solution)/shard_map/shi,hij->shj/dot_general | solution.py:142
  28.7 1.2 fusion.35
  29.9 0.3 slice_multiply_fusion.6
  30.2 0.4 slice_add_fusion.1
  30.6 0.2 slice.281
  30.8 0.2 bitcast_add_fusion
  32.3 0.4 broadcast_multiply_fusion
  32.7 1.2 copy.142
  34.0 0.1 copy-done.1
  34.1 1.2 copy.143
  35.4 0.6 broadcast_in_dim.19
  36.0 22.4 %all-to-all-start = ((f32[16,2,256]{2,1,0:T(2,128)}), f32[16,2,256]{2,1,0:T(2,128)S(1)}, u32[]{:S(2)}, u32[]{:S(2)}) async-start(f32[16,2,256]{2,1,0:T(2,128)} %broadcast_in_dim.19), calls=%async_computation | async-start | bytes 65536 | tf_op jit(solution)/shard_map/all_to_all | solution.py:15
  58.4 11.8 %all-to-all-done = f32[16,2,256]{2,1,0:T(2,128)S(1)} async-done(((f32[16,2,256]{2,1,0:T(2,128)}), f32[16,2,256]{2,1,0:T(2,128)S(1)}, u32[]{:S(2)}, u32[]{:S(2)}) %all-to-all-start) | async-done | bytes 32800 | tf_op jit(solution)/shard_map/all_to_all | solution.py:15
  70.6 10.5 %multiply_reduce_fusion = (f32[2048]{0:T(1024)S(1)}, f32[2048,256]{1,0:T(8,128)}) fusion(bf16[2048,256]{1,0:T(8,128)(2,1)S(1)} %copy-done, bf16[2048,2048]{1,0:T(8,128)(2,1)} %param.11, f32[2048]{0:T(1024)S(1)} %copy-done.9, f32[2048]{0:T(1024)S(1)} %add_rsqrt_fusion.1, f32[256]{0:T(256)S(1)} %bitcast.79, f32[256,8,256]{2,0,1:T(8,128)S(1)} %get-tuple-element.25, ...), kind=kOutput, calls=%fused_computation.42 | convolution fusion | flops 2172123136 | bytes 15754240 | tf_op jit(solution)/shard_map/dot_general | solution.py:130
  81.1 12.3 %all_to_all.30 = f32[8,1,2048]{2,1,0:T(1,128)S(1)} all-to-all(f32[8,1,2048]{2,1,0:T(1,128)S(1)} %broadcast_in_dim.22), channel_id=1, replica_groups=mesh['grp'=2,'sp'=16,'tp'=8] {'tp'}, dimensions={0} | all-to-all | bytes 131072 | tf_op jit(solution)/shard_map/all_to_all | solution.py:15
  93.4 2.0 %multiply_convert_fusion = bf16[2048,256]{1,0:T(8,128)(2,1)S(1)} fusion(f32[2048,256]{1,0:T(8,128)} %get-tuple-element.55, f32[256]{0:T(256)S(1)} %copy-done.5, f32[2048]{0:T(1024)S(1)} %add_rsqrt_fusion), kind=kLoop, calls=%fused_computation.41 | loop fusion | flops 1572864 | bytes 3154944 | tf_op jit(solution)/shard_map/convert_element_type | solution.py:155
  95.4 0.5 copy.84
  96.0 18.2 %all_to_all.31 = bf16[8,256,256]{1,2,0:T(8,128)(2,1)S(1)} all-to-all(bf16[8,256,256]{1,2,0:T(8,128)(2,1)S(1)} %copy.84), channel_id=1, replica_groups=mesh['grp'=2,'sp'=16,'tp'=8] {'tp'}, dimensions={0} | all-to-all | bytes 2097152 | tf_op jit(solution)/shard_map/all_to_all | solution.py:156
  114.1 14.9 %all-gather.2.cloned.1.call-done = bf16[2048,2048]{1,0:T(8,128)(2,1)} async-done(((bf16[128,2048]{1,0:T(8,128)(2,1)}), bf16[2048,2048]{1,0:T(8,128)(2,1)}) %all-gather.2.cloned.1.call-update) | async-done | bytes 8388624 | tf_op jit(solution)/shard_map/all_gather | solution.py:159
  129.0 6.7 %convolution_convert_fusion = bf16[256,2048]{1,0:T(8,128)(2,1)} fusion(bf16[256,2048]{0,1:T(8,128)(2,1)S(1)} %bitcast.64, bf16[2048,2048]{1,0:T(8,128)(2,1)} %all-gather.2.cloned.1.call-done), kind=kOutput, calls=%fused_computation.19 | convolution fusion | flops 2148007936 | bytes 10485760 | tf_op jit(solution)/shard_map/dot_general | solution.py:157
  (83 shorter events, 1.8 us)
Async XLA Ops:
  6.5 64.0 %copy-start = (bf16[2048,256]{1,0:T(8,128)(2,1)S(1)}, bf16[2048,256]{1,0:T(8,128)(2,1)}, u32[]{:S(2)}) copy-start(bf16[2048,256]{1,0:T(8,128)(2,1)} %param.14) | copy-start | bytes 3145732
  6.6 122.5 %all-gather.2.cloned.1.call-start = ((), (), s32[]{:S(2)}) async-start(), calls=%async_computation.3 | async-start | bytes 8912896 | tf_op jit(solution)/shard_map/all_gather | solution.py:159
  7.3 5.8 %copy-start.2 = (bf16[2048,2048]{1,0:T(8,128)(2,1)S(1)}, bf16[2048,2048]{1,0:T(8,128)(2,1)}, u32[]{:S(2)}) copy-start(bf16[2048,2048]{1,0:T(8,128)(2,1)} %param.11) | copy-start | bytes 25165828
  7.3 5.8 %copy-start.9 = (f32[2048]{0:T(1024)S(1)}, f32[2048]{0:T(1024)}, u32[]{:S(2)}) copy-start(f32[2048]{0:T(1024)} %param.12) | copy-start | bytes 24580
  13.1 9.4 %copy-start.4 = (f32[4,256]{1,0:T(4,128)S(1)}, f32[4,256]{1,0:T(4,128)}, u32[]{:S(2)}) copy-start(f32[4,256]{1,0:T(4,128)} %param.15) | copy-start | bytes 12292
  13.1 9.5 %copy-start.6 = (f32[256]{0:T(256)S(1)}, f32[256]{0:T(256)}, u32[]{:S(2)}) copy-start(f32[256]{0:T(256)} %param.18) | copy-start | bytes 3076
  13.1 10.0 %copy-start.3 = (f32[1,2048]{1,0:T(1,128)S(1)}, f32[1,2048]{1,0:T(1,128)}, u32[]{:S(2)}) copy-start(f32[1,2048]{1,0:T(1,128)} %param.19) | copy-start | bytes 24580
  17.1 6.8 %collective-permute-start = (bf16[3,256]{1,0:T(4,128)(2,1)S(1)}, bf16[3,256]{1,0:T(4,128)(2,1)S(1)}, u32[]{:S(2)}, u32[]{:S(2)}) collective-permute-start(bf16[3,256]{1,0:T(4,128)(2,1)S(1)} %slice.253), channel_id=1, source_target_pairs={{0,8},{8,16},{16,24},{24,32},{32,40},{40,48},{48,56},{56,64},{64,7... | collective-permute-start | bytes 4616 | tf_op jit(solution)/shard_map/ppermute | solution.py:10
  24.2 0.9 copy-start.7
  25.8 0.9 copy-start.8
  32.7 1.4 copy-start.1
  36.0 34.2 %all-to-all-start = ((f32[16,2,256]{2,1,0:T(2,128)}), f32[16,2,256]{2,1,0:T(2,128)S(1)}, u32[]{:S(2)}, u32[]{:S(2)}) async-start(f32[16,2,256]{2,1,0:T(2,128)} %broadcast_in_dim.19), calls=%async_computation | async-start | bytes 65536 | tf_op jit(solution)/shard_map/all_to_all | solution.py:15
  70.6 22.8 %copy-start.5 = (f32[256]{0:T(256)S(1)}, f32[256]{0:T(256)}, u32[]{:S(2)}) copy-start(f32[256]{0:T(256)} %param.20) | copy-start | bytes 3076
Sparse Core Ops, SparseCore 0:
  9.1 119.8 all-gather.1
where the time goes:
time: 143 us
  blocking collectives  30.4 us (21%)
  starting transfers between devices  27.8 us (19%)
  waiting for transfers between devices  27.4 us (19%)
  matrix products  23.8 us (17%)
  between operations  14 us (10%)
  other arithmetic  12 us (8%)
  local copies, waits for them, and re-layouts  7.12 us (5%)
    all_to_all x1, starting transfers between devices, sent_to_all(): return lax.all_to_all(copies, axis, split_axis=0, concat_axis=0, tiled=True)  22.4 us
    all_to_all x1, blocking collectives, body(): lax.all_to_all(normed_out, 'tp', split_axis=0, concat_axis=1, tiled=True)  18.2 us
    all_gather x1, waiting for transfers between devices, body(): lax.all_gather(w_out, 'sp', axis=0, tiled=True)  14.9 us
    all_to_all x1, blocking collectives, sent_to_all(): return lax.all_to_all(copies, axis, split_axis=0, concat_axis=0, tiled=True)  12.3 us
    all_to_all x1, waiting for transfers between devices, sent_to_all(): return lax.all_to_all(copies, axis, split_axis=0, concat_axis=0, tiled=True)  11.8 us
    dot_general x1, matrix products, body(): jnp.dot(normed, w_gate, preferred_element_type=jnp.float32)  10.5 us
    dot_general x1, matrix products, body(): jnp.dot(token_matrix, lax.all_gather(w_out, 'sp', axis=0, tiled=True), pr...  6.7 us
    ppermute x1, starting transfers between devices, from_behind(): return lax.ppermute(array, axis, pairs)  5.42 us
  transfers between devices with their start and end apart: 3, of which 2 were waited for; matrix products, arithmetic and copies ran while one was open for 25% of the time, Pallas kernels for 0%

commit v1 on v0

v1 whole, which is shorter than its diff:
```python
import functools

import jax
import jax.numpy as jnp
from jax import lax
from jax.experimental import pallas as pl
from jax.experimental.pallas import tpu as pltpu
from jax.sharding import PartitionSpec as P

MESH = pl.DeviceIdType.MESH
F32 = jnp.float32
BF16 = jnp.bfloat16
LANES = 128
SEGS = 8
STEP = 32
PAD = 40


def log1p_small(u):
    series = u * (1.0 - u * (0.5 - u * (1.0 / 3.0 - u * (0.25 - u * (0.2 - u / 6.0)))))
    return jnp.where(u < 0.06, series, jnp.log(1.0 + u))


def softplus(x):
    return jnp.maximum(x, 0.0) + log1p_small(jnp.exp(-jnp.abs(x)))


def gelu(x):
    inner = 0.7978845608028654 * (x + 0.044715 * (x * x * x))
    return 0.5 * x * (1.0 + jnp.tanh(inner))


def kernel(
    tokens_in,
    gain_in,
    w_input_in,
    w_gate_in,
    taps_in,
    w_rate_in,
    w_inlet_in,
    dparam_in,
    bias_in,
    ogain_in,
    w_out_in,
    out,
    tok,
    wi,
    wg,
    wrn,
    gain,
    taps,
    dparam,
    bias,
    ogain,
    wv,
    proj,
    halo,
    biasc,
    invc,
    conv,
    gates,
    sa,
    sb,
    ht,
    pt,
    ge,
    segh,
    segp,
    carry_own,
    carry,
    gout,
    grecv,
    ss_own,
    ss_recv,
    obuf,
    tok_sem,
    in_sem,
    wv_sem,
    out_sem,
    zr,
    xr,
    yr,
    zs,
    xs,
    ys,
    ds_send,
    ds_recv,
    halo_send,
    halo_recv,
    carry_send,
    carry_recv,
    a2a_send,
    a2a_recv,
    ss_send,
    ss_recv_sem,
    know,
):
    grp, z, tp = lax.axis_index("grp"), lax.axis_index("sp"), lax.axis_index("tp")
    spans, peers = lax.axis_size("sp"), lax.axis_size("tp")
    half = spans // 2
    core = lax.rem(tp, 2)
    rows, width = tok.shape
    channels = wi.shape[1]
    block = width // spans
    share = block // 2
    tile = rows // 4
    mine = rows // peers
    first = lax.rem(2 * (tp // 2) + 4 * lax.rem(grp, 2), 8)
    partner = grp + 1 - 2 * lax.rem(grp, 2)
    sibling = tp + 1 - 2 * core

    def column(pos):
        offset = (0, 1, 2, 3, 4, 6, 5, 7)[pos]
        return pl.multiple_of(lax.rem(first + offset, 8) * channels, channels)

    def local(src, dst, sem):
        return pltpu.make_async_copy(src, dst, sem)

    def remote(src, dst, send, recv, where):
        return pltpu.make_async_remote_copy(
            src_ref=src, dst_ref=dst, send_sem=send, recv_sem=recv, device_id=where, device_id_type=MESH
        )

    def lines_of(owner):
        return pl.ds(pl.multiple_of(owner * block + core * share, share), share)

    own_lines = pl.ds(pl.multiple_of(z * block, block), block)
    wv_copies = [
        local(w_out_in.at[:, pl.ds(column(pos), channels)], wv.at[pos, own_lines, :], wv_sem.at[pos])
        for pos in range(8)
    ]
    for pos in range(4):
        wv_copies[pos].start()
    in_copies = [
        local(gain_in, gain, in_sem.at[0]),
        local(w_input_in, wi, in_sem.at[1]),
        local(bias_in, bias, in_sem.at[2]),
        local(taps_in, taps, in_sem.at[3]),
        local(dparam_in, dparam, in_sem.at[4]),
        local(ogain_in, ogain, in_sem.at[5]),
        local(w_rate_in, wrn.at[:, 0:channels], in_sem.at[6]),
        local(w_inlet_in, wrn.at[:, channels : 2 * channels], in_sem.at[7]),
        local(w_gate_in, wg, in_sem.at[8]),
    ]
    for k in (0, 1, 2):
        in_copies[k].start()

    def tok_copy(k):
        part = pl.ds(pl.multiple_of(k * tile, tile), tile)
        return local(tokens_in.at[part, :], tok.at[part, :], tok_sem.at[k])

    for k in (3, 2, 1, 0):
        tok_copy(k).start()
    for k in range(3, 9):
        in_copies[k].start()
    for pos in range(4, 8):
        wv_copies[pos].start()

    barrier = pltpu.get_barrier_semaphore()
    above, below = lax.rem(z + 1, spans), lax.rem(z + spans - 1, spans)
    for where in (
        [{"sp": above}, {"sp": below}, {"grp": partner}]
        + [{"tp": lax.rem(tp + k, peers)} for k in range(1, 8)]
    ):
        pl.semaphore_signal(barrier, inc=1, device_id=where, device_id_type=MESH)
    pl.semaphore_wait(barrier, 10)

    def knowledge(level, distance):
        for other in (lax.rem(z + distance, spans), lax.rem(z + spans - distance, spans)):
            pl.semaphore_signal(know.at[level], inc=1, device_id={"sp": other}, device_id_type=MESH)

    knowledge(0, 1)

    def z_copy(way, u, owner):
        side = lax.rem(u, 2)
        part = wv.at[pl.ds(2 * side, 2), lines_of(owner), :]
        where = {"sp": above if way == 0 else below}
        return remote(part, part, zs, zr.at[way, u], where)

    def owner_of(way, u):
        t = u // 2 + 1
        return lax.rem(z + spans - t, spans) if way == 0 else lax.rem(z + t, spans)

    def x_copy(way, u):
        side = lax.rem(u, 2)
        lines = lines_of(owner_of(way, u))
        where = {"tp": lax.rem(tp + 2 + 4 * side, peers)}
        return remote(wv.at[1 + side, lines, :], wv.at[7 - 3 * side, lines, :], xs, xr.at[way, u], where)

    def y_copy(way, u):
        side = lax.rem(u, 2)
        lines = lines_of(owner_of(way, u))
        return remote(
            wv.at[1 + side, lines, :], wv.at[6 - side, lines, :], ys, yr.at[way, u], {"grp": partner}
        )

    def d_copy(way, u, start):
        part = wv.at[pl.ds(start, 2), lines_of(owner_of(way, u)), :]
        return remote(part, part, ds_send, ds_recv, {"tp": sibling})

    def ring(u, ways=(0, 1), forward=(0, 1)):
        side = lax.rem(u, 2)
        for way in ways:
            z_copy(way, u, owner_of(way, u)).wait_recv()
            if way in forward:
                z_copy(way, u + 2, owner_of(way, u)).start()
            x_copy(way, u).start()
            y_copy(way, u).start()
            d_copy(way, u, 2 * side).start()

    def spread(u, ways=(0, 1)):
        side = lax.rem(u, 2)
        for way in ways:
            x_copy(way, u).wait_recv()
            y_copy(way, u).wait_recv()
            d_copy(way, u, 6 - 2 * side).start()

    for pos in range(4):
        wv_copies[pos].wait()
    for u in (0, 1):
        for way in (0, 1):
            z_copy(way, u, z).start()

    in_copies[0].wait()
    in_copies[1].wait()
    in_copies[2].wait()
    gain_cols = gain[...].T
    bias_cols = bias[...].T
    for j in range(width // LANES):
        part = pl.ds(j * LANES, LANES)
        wi[part, :] = (wi[part, :].astype(F32) * gain_cols[:, j : j + 1]).astype(BF16)
        biasc[part, :] = jnp.broadcast_to(bias_cols[:, j : j + 1], (LANES, LANES))

    pl.semaphore_wait(know.at[0], 2)
    knowledge(1, 2)

    def halo_copy():
        return remote(proj.at[pl.ds(rows, 8), :], halo, halo_send, halo_recv, {"sp": above})

    def project(i, _):
        k = 3 - i
        base = pl.multiple_of(k * tile, tile)
        tok_copy(k).wait()

        def norms(j, _):
            part = pl.ds(pl.multiple_of(base + j * 64, 64), 64)
            total = jnp.zeros((64, LANES), F32)
            for c in range(width // LANES):
                x = tok[part, c * LANES : (c + 1) * LANES].astype(F32)
                total = total + x * x
            mean = jnp.sum(total, axis=1, keepdims=True) * (1.0 / width)
            invc[part, :] = jnp.broadcast_to(lax.rsqrt(mean + 1e-06), (64, LANES))
            return 0

        lax.fori_loop(0, tile // 64, norms, 0)
        part = pl.ds(base, tile)
        acc = jnp.dot(tok[part, :], wi[...], preferred_element_type=F32)
        inv = invc[part, :]
        for c in range(channels // LANES):
            lane = slice(c * LANES, (c + 1) * LANES)
            proj[pl.ds(base + 8, tile), lane] = (acc[:, lane] * inv).astype(BF16).astype(F32)

        @pl.when(i == 0)
        def _():
            halo_copy().start()

        return 0

    lax.fori_loop(0, 2, project, 0)
    pl.semaphore_wait(know.at[1], 2)
    knowledge(2, 4)
    ring(0)
    lax.fori_loop(2, 4, project, 0)
    ring(1)

    for k in range(3, 8):
        in_copies[k].wait()
    halo_copy().wait_recv()
    proj[0:8, :] = jnp.where(z > 0, halo[...], 0.0)

    scale = -8.0 * softplus(-dparam[...])
    tap = [taps[k : k + 1, :] for k in range(4)]

    def gather_inputs(i):
        for s in range(SEGS):
            base = pl.multiple_of(s * mine + i * STEP, STEP)
            x = proj[pl.ds(base, STEP + 8), :]
            total = pltpu.roll(x, 3, axis=0)[8:] * tap[0]
            total = total + pltpu.roll(x, 2, axis=0)[8:] * tap[1]
            total = total + pltpu.roll(x, 1, axis=0)[8:] * tap[2]
            total = total + x[8:] * tap[3]
            conv[s * STEP : (s + 1) * STEP, :] = total.astype(BF16)

    def scan_tile(i, state):
        gather_inputs(i)
        gates[...] = jnp.dot(conv[...], wrn[...], preferred_element_type=F32)
        for s in range(SEGS):
            base = pl.multiple_of(s * mine + i * STEP, STEP)
            shift = biasc[pl.ds(base, STEP), :]
            part = slice(s * STEP, (s + 1) * STEP)
            for c in range(channels // LANES):
                lane = slice(c * LANES, (c + 1) * LANES)
                rate = jax.nn.sigmoid(gates[part, lane])
                inlet = jax.nn.sigmoid(gates[part, channels + c * LANES : channels + (c + 1) * LANES])
                log_decay = rate * scale[:, lane] + shift
                decay = jnp.exp(log_decay)
                y = -2.0 * log_decay
                series = y * (
                    1.0 - y * (0.5 - y * (1.0 / 6.0 - y * (1.0 / 24.0 - y * (1.0 / 120.0))))
                )
                grown = jnp.where(y < 0.2, series, 1.0 - decay * decay)
                root = grown * lax.rsqrt(jnp.maximum(grown, 1e-37))
                drive = root * inlet * conv[part, lane].astype(F32)
                sa[c, s * PAD : s * PAD + STEP, :] = decay
                sb[c, s * PAD : s * PAD + STEP, :] = drive
        state = list(state)
        for r in range(STEP):
            line = pl.ds(pl.multiple_of((i * STEP + r) * SEGS, SEGS), SEGS)
            for c in range(channels // LANES):
                a = sa[c, pl.ds(r, SEGS, stride=PAD), :]
                b = sb[c, pl.ds(r, SEGS, stride=PAD), :]
                h, p = state[2 * c], state[2 * c + 1]
                h, p = a * h + b, a * p
                ht[c, line, :] = h
                pt[c, line, :] = p
                state[2 * c], state[2 * c + 1] = h, p
        return tuple(state)

    lanes2 = channels // LANES
    state = (jnp.zeros((SEGS, LANES), F32), jnp.ones((SEGS, LANES), F32)) * lanes2
    state = lax.fori_loop(0, 3, scan_tile, state)
    ring(2)
    spread(0)
    pl.semaphore_wait(know.at[2], 2)
    state = lax.fori_loop(3, 6, scan_tile, state)
    ring(3)
    spread(1)
    state = lax.fori_loop(6, 8, scan_tile, state)

    for c in range(lanes2):
        h_end, p_end = state[2 * c], state[2 * c + 1]
        h, p = jnp.zeros((1, LANES), F32), jnp.ones((1, LANES), F32)
        for s in range(SEGS):
            segh[c, s : s + 1, :] = h
            segp[c, s : s + 1, :] = p
            h = p_end[s : s + 1] * h + h_end[s : s + 1]
            p = p_end[s : s + 1] * p
        carry_own[c : c + 1, :] = p
        carry_own[lanes2 + c : lanes2 + c + 1, :] = h

    carry[z] = carry_own[...]
    for k in range(1, 16):
        other = lax.rem(z + k, spans)
        remote(carry_own, carry.at[z], carry_send, carry_recv, {"sp": other}).start()

    in_copies[8].wait()
    for j in range(width // LANES):
        part = pl.ds(j * LANES, LANES)
        wg[part, :] = (wg[part, :].astype(F32) * gain_cols[:, j : j + 1]).astype(BF16)

    def gate(i, _):
        part = pl.ds(pl.multiple_of(i * tile, tile), tile)
        acc = jnp.dot(tok[part, :], wg[...], preferred_element_type=F32)
        inv = invc[part, :]
        for c in range(lanes2):
            lane = slice(c * LANES, (c + 1) * LANES)
            ge[part, lane] = gelu((acc[:, lane] * inv).astype(BF16).astype(F32))
        return 0

    lax.fori_loop(0, 2, gate, 0)
    ring(4)
    spread(2)
    lax.fori_loop(2, 4, gate, 0)
    ring(5)
    spread(3)

    everyone = carry.at[pl.ds(0, 15)]
    local(everyone, everyone, carry_recv).wait()
    incoming = [jnp.zeros((1, LANES), F32) for _ in range(lanes2)]
    for j in range(15):
        for c in range(lanes2):
            p = carry[j, c : c + 1, :]
            h = carry[j, lanes2 + c : lanes2 + c + 1, :]
            incoming[c] = jnp.where(j < z, p * incoming[c] + h, incoming[c])

    def a2a_copy(other):
        return remote(gout.at[other], grecv.at[tp], a2a_send, a2a_recv.at[tp], {"tp": other})

    def ss_copy(other):
        return remote(ss_own.at[other], ss_recv.at[tp], ss_send, ss_recv_sem, {"tp": other})

    ones = jnp.ones((8, LANES), F32)

    def read_out(i, _):
        s = lax.rem(tp + 4 + i, peers)
        total = jnp.zeros((mine, LANES), F32)
        for c in range(lanes2):
            lane = slice(c * LANES, (c + 1) * LANES)
            enter = segp[c, pl.ds(s, 1), :] * incoming[c] + segh[c, pl.ds(s, 1), :]
            lines = pl.ds(s, mine, stride=SEGS)
            state = ht[c, lines, :] + pt[c, lines, :] * enter
            gated = state * ge[pl.ds(pl.multiple_of(s * mine, mine), mine), lane]
            total = total + gated * gated
            gout[s, :, lane] = (gated * ogain[:, lane]).astype(BF16)
        sums = lax.dot_general(
            ones, total, (((1,), (1,)), ((), ())), precision=lax.Precision.HIGHEST,
            preferred_element_type=F32,
        )
        ss_own[s] = sums[0:1, :]

        @pl.when(i != 4)
        def _():
            a2a_copy(s).start()
            ss_copy(s).start()

        return 0

    lax.fori_loop(0, 8, read_out, 0)
    grecv[tp] = gout[tp]
    ss_recv[tp] = ss_own[tp]

    for u in range(6, 12):
        ring(u)
        spread(u - 2)
    ring(12, forward=(0,))
    spread(10)
    ring(13, forward=(1,))
    spread(11)
    ring(14, ways=(0,), forward=())
    spread(12)
    ring(15, ways=(1,), forward=())
    spread(13)
    spread(14, ways=(0,))
    spread(15, ways=(1,))

    for pos in range(4, 8):
        wv_copies[pos].wait()
    for k in range(1, 8):
        other = lax.rem(tp + k, peers)
        remote(gout.at[other], grecv.at[other], a2a_send, a2a_recv.at[other], {"tp": other}).wait_recv()
    seven = ss_recv.at[pl.ds(0, 7)]
    local(seven, seven, ss_recv_sem).wait()
    everything = wv.at[:, pl.ds(0, 15 * share), :]
    local(everything, everything, ds_recv).wait()

    total = ss_recv[0]
    for k in range(1, 8):
        total = total + ss_recv[k]
    scales = lax.rsqrt(total * (1.0 / width) + 1e-06)
    scales = jnp.broadcast_to(scales, (LANES, mine)).T

    def finish(pos, _):
        acc = jnp.zeros((mine, channels), F32)
        for k in range(8):
            acc = acc + jnp.dot(
                grecv[k], wv[pos, k * channels : (k + 1) * channels, :], preferred_element_type=F32
            )
        for c in range(lanes2):
            lane = slice(c * LANES, (c + 1) * LANES)
            obuf[pos, :, lane] = (acc[:, lane] * scales).astype(BF16)
        return 0

    def out_copy(pos):
        return local(obuf.at[pos], out.at[:, pl.ds(column(pos), channels)], out_sem.at[pos])

    for pos in range(8):
        finish(pos, 0)
        out_copy(pos).start()

    sent = wv.at[pl.ds(0, 2), pl.ds(0, 30 * share), :]
    local(sent, sent, zs).wait()
    sent = wv.at[0, pl.ds(0, 30 * share), :]
    local(sent, sent, xs).wait()
    local(sent, sent, ys).wait()
    local(everything, everything, ds_send).wait()
    halo_copy().wait_send()
    local(everyone, everyone, carry_send).wait()
    sent = gout.at[pl.ds(0, 7)]
    local(sent, sent, a2a_send).wait()
    sent = ss_own.at[pl.ds(0, 7)]
    local(sent, sent, ss_send).wait()
    for pos in range(8):
        out_copy(pos).wait()


def body(
    tokens, in_gain, w_input, w_gate, conv_taps, w_rate, w_inlet, decay_param, decay_bias, out_gain, w_out
):
    rows, width = tokens.shape
    channels = w_input.shape[1]
    lanes2 = channels // LANES
    spans, peers = lax.axis_size("sp"), lax.axis_size("tp")
    mine = rows // peers
    vmem = pltpu.VMEM
    dma = pltpu.SemaphoreType.DMA
    scratch = [
        vmem((rows, width), BF16),
        vmem((width, channels), BF16),
        vmem((width, channels), BF16),
        vmem((channels, 2 * channels), BF16),
        vmem((width // LANES, LANES), F32),
        vmem((4, channels), F32),
        vmem((1, channels), F32),
        vmem((rows // LANES, LANES), F32),
        vmem((1, channels), F32),
        vmem((8, width, channels), BF16),
        vmem((8 + rows, channels), F32),
        vmem((8, channels), F32),
        vmem((rows, LANES), F32),
        vmem((rows, LANES), F32),
        vmem((SEGS * STEP, channels), BF16),
        vmem((SEGS * STEP, 2 * channels), F32),
        vmem((lanes2, SEGS * PAD, LANES), F32),
        vmem((lanes2, SEGS * PAD, LANES), F32),
        vmem((lanes2, rows, LANES), F32),
        vmem((lanes2, rows, LANES), F32),
        vmem((rows, channels), F32),
        vmem((lanes2, SEGS, LANES), F32),
        vmem((lanes2, SEGS, LANES), F32),
        vmem((2 * lanes2, LANES), F32),
        vmem((spans, 2 * lanes2, LANES), F32),
        vmem((peers, mine, channels), BF16),
        vmem((peers, mine, channels), BF16),
        vmem((peers, 1, mine), F32),
        vmem((peers, 1, mine), F32),
        vmem((8, mine, channels), BF16),
        dma((4,)),
        dma((9,)),
        dma((8,)),
        dma((8,)),
        dma((2, 16)),
        dma((2, 16)),
        dma((2, 16)),
    ] + [dma(())] * 10 + [dma((8,)), dma(()), dma(()), pltpu.SemaphoreType.REGULAR((3,))]
    spec = pl.BlockSpec(memory_space=pl.ANY)
    return pl.pallas_call(
        kernel,
        out_shape=jax.ShapeDtypeStruct((mine, width), BF16),
        in_specs=[spec] * 11,
        out_specs=spec,
        scratch_shapes=scratch,
        compiler_params=pltpu.CompilerParams(
            collective_id=0, has_side_effects=True, vmem_limit_bytes=60 * 1024 * 1024
        ),
        name="gated_recurrence",
    )(
        tokens,
        in_gain.reshape(width // LANES, LANES),
        w_input,
        w_gate,
        conv_taps,
        w_rate.reshape(channels, channels),
        w_inlet.reshape(channels, channels),
        decay_param.reshape(1, channels),
        decay_bias.reshape(rows // LANES, LANES),
        out_gain.reshape(1, channels),
        w_out,
    )


def solution(mesh):
    return jax.shard_map(
        body,
        mesh=mesh,
        in_specs=(
            P(("grp", "sp"), None),
            P(),
            P(None, "tp"),
            P(None, "tp"),
            P(None, "tp"),
            P("tp", None, None),
            P("tp", None, None),
            P("tp"),
            P("tp", ("grp", "sp")),
            P("tp"),
            P("sp", None),
        ),
        out_specs=P(("grp", "sp", "tp"), None),
        check_vma=False,
    )
```

time: 143 us -> 82 us (0.57)
  Pallas kernels: 0 us -> 79.5 us
  blocking collectives: 30.4 us -> 0 us
  starting transfers between devices: 27.8 us -> 0 us
  waiting for transfers between devices: 27.4 us -> 0 us
  matrix products: 23.8 us -> 0 us
  between operations: 14 us -> 0.01 us
  other arithmetic: 12 us -> 0 us
  local copies, waits for them, and re-layouts: 7.12 us -> 2.3 us
    pallas_call x0 -> x1, Pallas kernels: none -> 79.5 us  [body(): pl.pallas_call(kernel, out_shape=jax.ShapeDtypeStruct((mine, width), BF16...]
    all_to_all x2 -> x0, blocking collectives: 30.4 us -> none  [the longest x1 18.2 us: body(): lax.all_to_all(normed_out, 'tp', split_axis=0, concat_axis=1, tiled=True)]
    dot_general x5 -> x0, matrix products: 23.8 us -> none  [the longest x1 10.5 us: body(): jnp.dot(normed, w_gate, preferred_element_type=jnp.float32)]
    all_to_all x1 -> x0, starting transfers between devices: 22.4 us -> none  [sent_to_all(): return lax.all_to_all(copies, axis, split_axis=0, concat_axis=0, tiled=True)]
    all_gather x1 -> x0, waiting for transfers between devices: 14.9 us -> none  [body(): lax.all_gather(w_out, 'sp', axis=0, tiled=True)]
    all_to_all x1 -> x0, waiting for transfers between devices: 11.8 us -> none  [sent_to_all(): return lax.all_to_all(copies, axis, split_axis=0, concat_axis=0, tiled=True)]
    ppermute x1 -> x0, starting transfers between devices: 5.42 us -> none  [from_behind(): return lax.ppermute(array, axis, pairs)]
    reduce_sum x2 -> x0, other arithmetic: 5.29 us -> none  [the longest x1 5.23 us: body(): jnp.mean(as_float * as_float, axis=1, keepdims=True) + 1e-06]
  transfers between devices with their start and end apart: 3 -> 0, of which waited for: 2 -> 0; matrix products, arithmetic and copies ran while one was open for 25% -> 0% of each run, Pallas kernels for 0% -> 0%
where the time goes in v1:
time: 82 us; the launch traced here: 81.8 us
  Pallas kernels  79.5 us (97%)
  local copies, waits for them, and re-layouts  2.3 us (3%)
    pallas_call x1, Pallas kernels, body(): pl.pallas_call(kernel, out_shape=jax.ShapeDtypeStruct((mine, width), BF16...  79.5 us
    unnamed x1, local copies, waits for them, and re-layouts  2.3 us

profile of v1, /device:TPU:33, one launch (start us, length us, event | category | flops | bytes accessed | tf_op | source)
XLA Modules:
  0.0 81.8 jit_solution(6920247684972347223)
XLA Ops:
  0.0 79.5 %gated_recurrence.1 = bf16[256,2048]{1,0:T(8,128)(2,1)} custom-call(bf16[2048,2048]{1,0:T(8,128)(2,1)} %tokens_in.1, f32[16,128]{1,0:T(8,128)} %bitcast.8, bf16[2048,256]{1,0:T(8,128)(2,1)} %w_input_in.1, bf16[2048,256]{1,0:T(8,128)(2,1)} %w_gate_in.1, f32[4,256]{1,0:T(4,128)} %taps_in.1, bf16[256,256]{1,0:T(8,128)(2,1)} %bitcast.6, ...), custom_call_target="tpu_custom_call" | custom-call | tf_op jit(solution)/shard_map/gated_recurrence/pallas_call | solution.py:536
  79.5 2.3 %copy.13 = bf16[256,2048]{1,0:T(8,128)(2,1)} copy(bf16[256,2048]{1,0:T(8,128)(2,1)} %gated_recurrence.1) | data formatting | bytes 2097152

commit v2 on v1

--- a/solution.py
+++ b/solution.py
@@ -67,6 +67,7 @@
     segh,
     segp,
     carry_own,
+    state_own,
     carry,
     gout,
     grecv,
@@ -77,10 +78,10 @@
     in_sem,
     wv_sem,
     out_sem,
+    zs,
     zr,
     xr,
     yr,
-    zs,
     xs,
     ys,
     ds_send,
@@ -97,7 +98,6 @@
 ):
     grp, z, tp = lax.axis_index("grp"), lax.axis_index("sp"), lax.axis_index("tp")
     spans, peers = lax.axis_size("sp"), lax.axis_size("tp")
-    half = spans // 2
     core = lax.rem(tp, 2)
     rows, width = tok.shape
     channels = wi.shape[1]
@@ -110,8 +110,7 @@
     sibling = tp + 1 - 2 * core
 
     def column(pos):
-        offset = (0, 1, 2, 3, 4, 6, 5, 7)[pos]
-        return pl.multiple_of(lax.rem(first + offset, 8) * channels, channels)
+        return pl.multiple_of(lax.rem(first + pos, 8) * channels, channels)
 
     def local(src, dst, sem):
         return pltpu.make_async_copy(src, dst, sem)
@@ -129,7 +128,7 @@
         local(w_out_in.at[:, pl.ds(column(pos), channels)], wv.at[pos, own_lines, :], wv_sem.at[pos])
         for pos in range(8)
     ]
-    for pos in range(4):
+    for pos in range(2):
         wv_copies[pos].start()
     in_copies = [
         local(gain_in, gain, in_sem.at[0]),
@@ -153,73 +152,95 @@
         tok_copy(k).start()
     for k in range(3, 9):
         in_copies[k].start()
-    for pos in range(4, 8):
+    for pos in range(2, 8):
         wv_copies[pos].start()
 
+    last = spans - 1
     barrier = pltpu.get_barrier_semaphore()
-    above, below = lax.rem(z + 1, spans), lax.rem(z + spans - 1, spans)
-    for where in (
-        [{"sp": above}, {"sp": below}, {"grp": partner}]
-        + [{"tp": lax.rem(tp + k, peers)} for k in range(1, 8)]
-    ):
+    above, below = lax.rem(z + 1, spans), lax.rem(z + last, spans)
+    for where in [{"grp": partner}] + [{"tp": lax.rem(tp + k, peers)} for k in range(1, 8)]:
         pl.semaphore_signal(barrier, inc=1, device_id=where, device_id_type=MESH)
-    pl.semaphore_wait(barrier, 10)
-
-    def knowledge(level, distance):
-        for other in (lax.rem(z + distance, spans), lax.rem(z + spans - distance, spans)):
-            pl.semaphore_signal(know.at[level], inc=1, device_id={"sp": other}, device_id_type=MESH)
-
-    knowledge(0, 1)
-
-    def z_copy(way, u, owner):
-        side = lax.rem(u, 2)
-        part = wv.at[pl.ds(2 * side, 2), lines_of(owner), :]
+
+    def tell(sem, other):
+        pl.semaphore_signal(sem, inc=1, device_id={"sp": other}, device_id_type=MESH)
+
+    pl.when(z < last)(lambda: tell(barrier, above))
+    pl.when(z > 0)(lambda: tell(barrier, below))
+    ends = jnp.where(z > 0, 1, 0) + jnp.where(z < last, 1, 0)
+    pl.semaphore_wait(barrier, 8 + ends)
+
+    def learn(level):
+        pl.when(z < last)(lambda: pl.semaphore_wait(know.at[level], 1))
+
+    def teach(level):
+        pl.when(z > 0)(lambda: tell(know.at[level], below))
+
+    teach(0)
+    pl.when(z > 0)(lambda: pl.semaphore_wait(know.at[3], 1))
+    pl.when(z < last)(lambda: tell(know.at[3], above))
+    pl.when(z == last)(lambda: tell(know.at[4], above))
+
+    def from_below(span):
+        return jnp.minimum(span, 2) + 6
+
+    def from_above(span):
+        return 9 - jnp.minimum(span, 2)
+
+    def z_copy(way, t, side, owner):
+        part = wv.at[side, lines_of(owner), :]
         where = {"sp": above if way == 0 else below}
-        return remote(part, part, zs, zr.at[way, u], where)
-
-    def owner_of(way, u):
-        t = u // 2 + 1
+        return remote(part, part, zs.at[way, t, side], zr.at[way, t, side], where)
+
+    def owner_of(way, t):
         return lax.rem(z + spans - t, spans) if way == 0 else lax.rem(z + t, spans)
 
-    def x_copy(way, u):
-        side = lax.rem(u, 2)
-        lines = lines_of(owner_of(way, u))
-        where = {"tp": lax.rem(tp + 2 + 4 * side, peers)}
-        return remote(wv.at[1 + side, lines, :], wv.at[7 - 3 * side, lines, :], xs, xr.at[way, u], where)
-
-    def y_copy(way, u):
-        side = lax.rem(u, 2)
-        lines = lines_of(owner_of(way, u))
-        return remote(
-            wv.at[1 + side, lines, :], wv.at[6 - side, lines, :], ys, yr.at[way, u], {"grp": partner}
-        )
-
-    def d_copy(way, u, start):
-        part = wv.at[pl.ds(start, 2), lines_of(owner_of(way, u)), :]
+    def share_copy(k, way, t):
+        lines = lines_of(owner_of(way, t))
+        part = wv.at[0:2, lines, :]
+        if k == 0:
+            where = {"tp": lax.rem(tp + 2, peers)}
+            return remote(part, wv.at[6:8, lines, :], xs, xr.at[0, way, t], where)
+        if k == 1:
+            where = {"tp": lax.rem(tp + 6, peers)}
+            return remote(part, wv.at[2:4, lines, :], xs, xr.at[1, way, t], where)
+        if k == 2:
+            return remote(part, wv.at[4:6, lines, :], ys, yr.at[way, t], {"grp": partner})
         return remote(part, part, ds_send, ds_recv, {"tp": sibling})
 
-    def ring(u, ways=(0, 1), forward=(0, 1)):
-        side = lax.rem(u, 2)
-        for way in ways:
-            z_copy(way, u, owner_of(way, u)).wait_recv()
-            if way in forward:
-                z_copy(way, u + 2, owner_of(way, u)).start()
-            x_copy(way, u).start()
-            y_copy(way, u).start()
-            d_copy(way, u, 2 * side).start()
-
-    def spread(u, ways=(0, 1)):
-        side = lax.rem(u, 2)
-        for way in ways:
-            x_copy(way, u).wait_recv()
-            y_copy(way, u).wait_recv()
-            d_copy(way, u, 6 - 2 * side).start()
-
-    for pos in range(4):
+    def ring(way, t):
+        owner = owner_of(way, t)
+        if way == 0:
+            more = t + 1 <= from_below(above)
+        else:
+            more = jnp.logical_and(z > 0, t + 1 <= from_above(below))
+        for side in (0, 1):
+            z_copy(way, t, side, owner).wait_recv()
+
+            @pl.when(more)
+            def _():
+                z_copy(way, t + 1, side, owner).start()
+
+        for k in range(4):
+            share_copy(k, way, t).start()
+
+    def spread(way, t):
+        for k in range(3):
+            share_copy(k, way, t).wait_recv()
+        part = wv.at[2:8, lines_of(owner_of(way, t)), :]
+        remote(part, part, ds_send, ds_recv, {"tp": sibling}).start()
+
+    def early(act, t):
+        pl.when(z >= t)(lambda: act(0, t))
+
+    for pos in range(2):
         wv_copies[pos].wait()
-    for u in (0, 1):
-        for way in (0, 1):
-            z_copy(way, u, z).start()
+
+    def first_sends(way):
+        for side in (0, 1):
+            z_copy(way, 1, side, z).start()
+
+    first_sends(0)
+    pl.when(z > 0)(lambda: first_sends(1))
 
     in_copies[0].wait()
     in_copies[1].wait()
@@ -231,9 +252,6 @@
         wi[part, :] = (wi[part, :].astype(F32) * gain_cols[:, j : j + 1]).astype(BF16)
         biasc[part, :] = jnp.broadcast_to(bias_cols[:, j : j + 1], (LANES, LANES))
 
-    pl.semaphore_wait(know.at[0], 2)
-    knowledge(1, 2)
-
     def halo_copy():
         return remote(proj.at[pl.ds(rows, 8), :], halo, halo_send, halo_recv, {"sp": above})
 
@@ -260,23 +278,34 @@
             lane = slice(c * LANES, (c + 1) * LANES)
             proj[pl.ds(base + 8, tile), lane] = (acc[:, lane] * inv).astype(BF16).astype(F32)
 
-        @pl.when(i == 0)
+        @pl.when(jnp.logical_and(i == 0, z < last))
         def _():
             halo_copy().start()
 
         return 0
 
     lax.fori_loop(0, 2, project, 0)
-    pl.semaphore_wait(know.at[1], 2)
-    knowledge(2, 4)
-    ring(0)
+    learn(0)
+    teach(1)
+    early(ring, 1)
     lax.fori_loop(2, 4, project, 0)
-    ring(1)
+    learn(1)
+    teach(2)
+    ring(1, 1)
+    early(ring, 2)
+    early(spread, 1)
 
     for k in range(3, 8):
         in_copies[k].wait()
-    halo_copy().wait_recv()
-    proj[0:8, :] = jnp.where(z > 0, halo[...], 0.0)
+    pl.when(z > 0)(lambda: halo_copy().wait_recv())
+
+    @pl.when(z > 0)
+    def _():
+        proj[0:8, :] = halo[...]
+
+    @pl.when(z == 0)
+    def _():
+        proj[0:8, :] = jnp.zeros((8, channels), F32)
 
     scale = -8.0 * softplus(-dparam[...])
     tap = [taps[k : k + 1, :] for k in range(4)]
@@ -329,12 +358,13 @@
     lanes2 = channels // LANES
     state = (jnp.zeros((SEGS, LANES), F32), jnp.ones((SEGS, LANES), F32)) * lanes2
     state = lax.fori_loop(0, 3, scan_tile, state)
-    ring(2)
-    spread(0)
-    pl.semaphore_wait(know.at[2], 2)
+    early(ring, 3)
+    early(spread, 2)
+    spread(1, 1)
     state = lax.fori_loop(3, 6, scan_tile, state)
-    ring(3)
-    spread(1)
+    ring(1, 2)
+    early(ring, 4)
+    early(spread, 3)
     state = lax.fori_loop(6, 8, scan_tile, state)
 
     for c in range(lanes2):
@@ -348,10 +378,16 @@
         carry_own[c : c + 1, :] = p
         carry_own[lanes2 + c : lanes2 + c + 1, :] = h
 
-    carry[z] = carry_own[...]
-    for k in range(1, 16):
-        other = lax.rem(z + k, spans)
-        remote(carry_own, carry.at[z], carry_send, carry_recv, {"sp": other}).start()
+    learn(2)
+
+    def carry_copy(k):
+        return remote(
+            carry_own, carry.at[k - 1], carry_send.at[k - 1], carry_recv.at[k - 1],
+            {"sp": lax.rem(z + k, spans)},
+        )
+
+    for k in (1, 2, 3):
+        pl.when(z + k < spans)(lambda: carry_copy(k).start())
 
     in_copies[8].wait()
     for j in range(width // LANES):
@@ -368,20 +404,39 @@
         return 0
 
     lax.fori_loop(0, 2, gate, 0)
-    ring(4)
-    spread(2)
+    early(ring, 5)
+    early(spread, 4)
+    spread(1, 2)
     lax.fori_loop(2, 4, gate, 0)
-    ring(5)
-    spread(3)
-
-    everyone = carry.at[pl.ds(0, 15)]
-    local(everyone, everyone, carry_recv).wait()
-    incoming = [jnp.zeros((1, LANES), F32) for _ in range(lanes2)]
-    for j in range(15):
-        for c in range(lanes2):
-            p = carry[j, c : c + 1, :]
-            h = carry[j, lanes2 + c : lanes2 + c + 1, :]
-            incoming[c] = jnp.where(j < z, p * incoming[c] + h, incoming[c])
+    ring(1, 3)
+    early(ring, 6)
+    early(spread, 5)
+
+    def state_copy():
+        return remote(
+            state_own, carry.at[3], carry_send.at[3], carry_recv.at[3], {"sp": lax.rem(z + 4, spans)}
+        )
+
+    def received(copy, slot, k):
+        pl.when(z >= k)(lambda: copy.wait_recv())
+
+        @pl.when(z < k)
+        def _():
+            carry[slot] = jnp.zeros(carry.shape[1:], F32)
+
+    received(state_copy(), 3, 4)
+    for k in (1, 2, 3):
+        received(carry_copy(k), k - 1, k)
+    incoming = []
+    for c in range(lanes2):
+        h = carry[3, lanes2 + c : lanes2 + c + 1, :]
+        for k in (3, 2, 1):
+            h = carry[k - 1, c : c + 1, :] * h + carry[k - 1, lanes2 + c : lanes2 + c + 1, :]
+        incoming.append(h)
+        out_state = carry_own[c : c + 1, :] * h + carry_own[lanes2 + c : lanes2 + c + 1, :]
+        state_own[c : c + 1, :] = jnp.zeros((1, LANES), F32)
+        state_own[lanes2 + c : lanes2 + c + 1, :] = out_state
+    pl.when(z + 4 < spans)(lambda: state_copy().start())
 
     def a2a_copy(other):
         return remote(gout.at[other], grecv.at[tp], a2a_send, a2a_recv.at[tp], {"tp": other})
@@ -419,21 +474,58 @@
     grecv[tp] = gout[tp]
     ss_recv[tp] = ss_own[tp]
 
-    for u in range(6, 12):
-        ring(u)
-        spread(u - 2)
-    ring(12, forward=(0,))
-    spread(10)
-    ring(13, forward=(1,))
-    spread(11)
-    ring(14, ways=(0,), forward=())
-    spread(12)
-    ring(15, ways=(1,), forward=())
-    spread(13)
-    spread(14, ways=(0,))
-    spread(15, ways=(1,))
-
-    for pos in range(4, 8):
+    done = jnp.minimum(z, 8)
+
+    def late(act, k):
+        pl.when(done + k <= from_below(z))(lambda: act(0, done + k))
+
+    def upper(act, t):
+        pl.when(t <= from_above(z))(lambda: act(1, t))
+
+    early(ring, 7)
+    early(ring, 8)
+    ring(1, 4)
+    early(spread, 6)
+    spread(1, 3)
+    early(spread, 7)
+    ring(1, 5)
+    early(spread, 8)
+    spread(1, 4)
+
+    def to_last(t, _):
+        for side in (0, 1):
+            z_copy(1, t + 1, side, t).start()
+        return 0
+
+    @pl.when(z == 0)
+    def _():
+        pl.semaphore_wait(know.at[4], 1)
+        lax.fori_loop(0, 6, to_last, 0)
+
+    ring(1, 6)
+    pl.when(z == 0)(lambda: (to_last(6, 0), None)[1])
+    spread(1, 5)
+    late(ring, 1)
+    late(ring, 2)
+    spread(1, 6)
+    ring(1, 7)
+    late(spread, 1)
+    late(ring, 3)
+    late(spread, 2)
+    late(ring, 4)
+    spread(1, 7)
+    upper(ring, 8)
+    late(spread, 3)
+    late(ring, 5)
+    late(spread, 4)
+    upper(ring, 9)
+    upper(spread, 8)
+    late(ring, 6)
+    late(spread, 5)
+    upper(spread, 9)
+    late(spread, 6)
+
+    for pos in range(2, 8):
         wv_copies[pos].wait()
     for k in range(1, 8):
         other = lax.rem(tp + k, peers)
@@ -467,14 +559,24 @@
         finish(pos, 0)
         out_copy(pos).start()
 
-    sent = wv.at[pl.ds(0, 2), pl.ds(0, 30 * share), :]
-    local(sent, sent, zs).wait()
-    sent = wv.at[0, pl.ds(0, 30 * share), :]
-    local(sent, sent, xs).wait()
-    local(sent, sent, ys).wait()
+    for way in (0, 1):
+        count = from_below(above) if way == 0 else from_above(below)
+
+        def sent(t, _):
+            for side in (0, 1):
+                z_copy(way, t + 1, side, z).wait_send()
+            return 0
+
+        lax.fori_loop(0, count, sent, 0)
+    shared = wv.at[0:4, pl.ds(0, 15 * share), :]
+    local(shared, shared, xs).wait()
+    shared = wv.at[0:2, pl.ds(0, 15 * share), :]
+    local(shared, shared, ys).wait()
     local(everything, everything, ds_send).wait()
-    halo_copy().wait_send()
-    local(everyone, everyone, carry_send).wait()
+    pl.when(z < last)(lambda: halo_copy().wait_send())
+    for k in (1, 2, 3):
+        pl.when(z + k < spans)(lambda: carry_copy(k).wait_send())
+    pl.when(z + 4 < spans)(lambda: state_copy().wait_send())
     sent = gout.at[pl.ds(0, 7)]
     local(sent, sent, a2a_send).wait()
     sent = ss_own.at[pl.ds(0, 7)]
@@ -518,7 +620,8 @@
         vmem((lanes2, SEGS, LANES), F32),
         vmem((lanes2, SEGS, LANES), F32),
         vmem((2 * lanes2, LANES), F32),
-        vmem((spans, 2 * lanes2, LANES), F32),
+        vmem((2 * lanes2, LANES), F32),
+        vmem((4, 2 * lanes2, LANES), F32),
         vmem((peers, mine, channels), BF16),
         vmem((peers, mine, channels), BF16),
         vmem((peers, 1, mine), F32),
@@ -528,10 +631,13 @@
         dma((9,)),
         dma((8,)),
         dma((8,)),
-        dma((2, 16)),
-        dma((2, 16)),
-        dma((2, 16)),
-    ] + [dma(())] * 10 + [dma((8,)), dma(()), dma(()), pltpu.SemaphoreType.REGULAR((3,))]
+        dma((2, 10, 2)),
+        dma((2, 10, 2)),
+        dma((2, 2, 10)),
+        dma((2, 10)),
+    ]
+    scratch += [dma(())] * 6 + [dma((4,)), dma((4,)), dma(()), dma((8,)), dma(()), dma(())]
+    scratch += [pltpu.SemaphoreType.REGULAR((5,))]
     spec = pl.BlockSpec(memory_space=pl.ANY)
     return pl.pallas_call(
         kernel,

time: 82 us -> 90 us (1.098)
  the two profiles are of different devices: /device:TPU:33 before, /device:TPU:1825 now
where the time goes in v2:
time: 90 us; the launch traced here: 89.8 us
  Pallas kernels  87.5 us (97%)
  local copies, waits for them, and re-layouts  2.3 us (3%)
    pallas_call x1, Pallas kernels, body(): pl.pallas_call(kernel, out_shape=jax.ShapeDtypeStruct((mine, width), BF16...  87.5 us
    unnamed x1, local copies, waits for them, and re-layouts  2.3 us

profile of v2, /device:TPU:1825, one launch (start us, length us, event | category | flops | bytes accessed | tf_op | source)
XLA Modules:
  0.0 89.8 jit_solution(674024005789804798)
XLA Ops:
  0.0 87.5 %gated_recurrence.1 = bf16[256,2048]{1,0:T(8,128)(2,1)} custom-call(bf16[2048,2048]{1,0:T(8,128)(2,1)} %tokens_in.1, f32[16,128]{1,0:T(8,128)} %bitcast.8, bf16[2048,256]{1,0:T(8,128)(2,1)} %w_input_in.1, bf16[2048,256]{1,0:T(8,128)(2,1)} %w_gate_in.1, f32[4,256]{1,0:T(4,128)} %taps_in.1, bf16[256,256]{1,0:T(8,128)(2,1)} %bitcast.6, ...), custom_call_target="tpu_custom_call" | custom-call | tf_op jit(solution)/shard_map/gated_recurrence/pallas_call | solution.py:642
  87.5 2.3 %copy.13 = bf16[256,2048]{1,0:T(8,128)(2,1)} copy(bf16[256,2048]{1,0:T(8,128)(2,1)} %gated_recurrence.1) | data formatting | bytes 2097152

commit v3 on v2

--- a/solution.py
+++ b/solution.py
@@ -101,6 +101,7 @@
     core = lax.rem(tp, 2)
     rows, width = tok.shape
     channels = wi.shape[1]
+    lanes2 = channels // LANES
     block = width // spans
     share = block // 2
     tile = rows // 4
@@ -158,33 +159,30 @@
     last = spans - 1
     barrier = pltpu.get_barrier_semaphore()
     above, below = lax.rem(z + 1, spans), lax.rem(z + last, spans)
-    for where in [{"grp": partner}] + [{"tp": lax.rem(tp + k, peers)} for k in range(1, 8)]:
+    for where in (
+        [{"sp": above}, {"sp": below}, {"grp": partner}]
+        + [{"tp": lax.rem(tp + k, peers)} for k in range(1, 8)]
+    ):
         pl.semaphore_signal(barrier, inc=1, device_id=where, device_id_type=MESH)
-
-    def tell(sem, other):
-        pl.semaphore_signal(sem, inc=1, device_id={"sp": other}, device_id_type=MESH)
-
-    pl.when(z < last)(lambda: tell(barrier, above))
-    pl.when(z > 0)(lambda: tell(barrier, below))
-    ends = jnp.where(z > 0, 1, 0) + jnp.where(z < last, 1, 0)
-    pl.semaphore_wait(barrier, 8 + ends)
+    pl.semaphore_wait(barrier, 10)
 
     def learn(level):
         pl.when(z < last)(lambda: pl.semaphore_wait(know.at[level], 1))
 
     def teach(level):
-        pl.when(z > 0)(lambda: tell(know.at[level], below))
+        @pl.when(z > 0)
+        def _():
+            pl.semaphore_signal(know.at[level], inc=1, device_id={"sp": below}, device_id_type=MESH)
 
     teach(0)
-    pl.when(z > 0)(lambda: pl.semaphore_wait(know.at[3], 1))
-    pl.when(z < last)(lambda: tell(know.at[3], above))
-    pl.when(z == last)(lambda: tell(know.at[4], above))
+
+    place = below
 
     def from_below(span):
-        return jnp.minimum(span, 2) + 6
+        return jnp.minimum(lax.rem(span + last, spans), 2) + 6
 
     def from_above(span):
-        return 9 - jnp.minimum(span, 2)
+        return 9 - jnp.minimum(lax.rem(span + last, spans), 2)
 
     def z_copy(way, t, side, owner):
         part = wv.at[side, lines_of(owner), :]
@@ -209,10 +207,7 @@
 
     def ring(way, t):
         owner = owner_of(way, t)
-        if way == 0:
-            more = t + 1 <= from_below(above)
-        else:
-            more = jnp.logical_and(z > 0, t + 1 <= from_above(below))
+        more = t + 1 <= (from_below(above) if way == 0 else from_above(below))
         for side in (0, 1):
             z_copy(way, t, side, owner).wait_recv()
 
@@ -230,7 +225,7 @@
         remote(part, part, ds_send, ds_recv, {"tp": sibling}).start()
 
     def early(act, t):
-        pl.when(z >= t)(lambda: act(0, t))
+        pl.when(place > t)(lambda: act(0, t))
 
     for pos in range(2):
         wv_copies[pos].wait()
@@ -240,7 +235,7 @@
             z_copy(way, 1, side, z).start()
 
     first_sends(0)
-    pl.when(z > 0)(lambda: first_sends(1))
+    first_sends(1)
 
     in_copies[0].wait()
     in_copies[1].wait()
@@ -260,23 +255,21 @@
         base = pl.multiple_of(k * tile, tile)
         tok_copy(k).wait()
 
-        def norms(j, _):
-            part = pl.ds(pl.multiple_of(base + j * 64, 64), 64)
+        part = pl.ds(base, tile)
+        acc = jnp.dot(tok[part, :], wi[...], preferred_element_type=F32)
+        for j in range(tile // 64):
+            lines = pl.ds(pl.multiple_of(base + j * 64, 64), 64)
             total = jnp.zeros((64, LANES), F32)
             for c in range(width // LANES):
-                x = tok[part, c * LANES : (c + 1) * LANES].astype(F32)
+                x = tok[lines, c * LANES : (c + 1) * LANES].astype(F32)
                 total = total + x * x
             mean = jnp.sum(total, axis=1, keepdims=True) * (1.0 / width)
-            invc[part, :] = jnp.broadcast_to(lax.rsqrt(mean + 1e-06), (64, LANES))
-            return 0
-
-        lax.fori_loop(0, tile // 64, norms, 0)
-        part = pl.ds(base, tile)
-        acc = jnp.dot(tok[part, :], wi[...], preferred_element_type=F32)
-        inv = invc[part, :]
-        for c in range(channels // LANES):
-            lane = slice(c * LANES, (c + 1) * LANES)
-            proj[pl.ds(base + 8, tile), lane] = (acc[:, lane] * inv).astype(BF16).astype(F32)
+            inv = jnp.broadcast_to(lax.rsqrt(mean + 1e-06), (64, LANES))
+            invc[lines, :] = inv
+            for c in range(lanes2):
+                lane = slice(c * LANES, (c + 1) * LANES)
+                scaled = acc[j * 64 : (j + 1) * 64, lane] * inv
+                proj[pl.ds(base + 8 + j * 64, 64), lane] = scaled.astype(BF16).astype(F32)
 
         @pl.when(jnp.logical_and(i == 0, z < last))
         def _():
@@ -293,7 +286,6 @@
     teach(2)
     ring(1, 1)
     early(ring, 2)
-    early(spread, 1)
 
     for k in range(3, 8):
         in_copies[k].wait()
@@ -355,16 +347,14 @@
                 state[2 * c], state[2 * c + 1] = h, p
         return tuple(state)
 
-    lanes2 = channels // LANES
     state = (jnp.zeros((SEGS, LANES), F32), jnp.ones((SEGS, LANES), F32)) * lanes2
     state = lax.fori_loop(0, 3, scan_tile, state)
     early(ring, 3)
-    early(spread, 2)
-    spread(1, 1)
     state = lax.fori_loop(3, 6, scan_tile, state)
     ring(1, 2)
     early(ring, 4)
-    early(spread, 3)
+    early(spread, 1)
+    spread(1, 1)
     state = lax.fori_loop(6, 8, scan_tile, state)
 
     for c in range(lanes2):
@@ -405,12 +395,13 @@
 
     lax.fori_loop(0, 2, gate, 0)
     early(ring, 5)
-    early(spread, 4)
-    spread(1, 2)
+    early(spread, 2)
+    early(spread, 3)
     lax.fori_loop(2, 4, gate, 0)
     ring(1, 3)
     early(ring, 6)
-    early(spread, 5)
+    spread(1, 2)
+    early(spread, 4)
 
     def state_copy():
         return remote(
@@ -474,7 +465,7 @@
     grecv[tp] = gout[tp]
     ss_recv[tp] = ss_own[tp]
 
-    done = jnp.minimum(z, 8)
+    done = jnp.clip(place - 1, 0, 8)
 
     def late(act, k):
         pl.when(done + k <= from_below(z))(lambda: act(0, done + k))
@@ -485,45 +476,36 @@
     early(ring, 7)
     early(ring, 8)
     ring(1, 4)
+    late(ring, 1)
+    ring(1, 5)
+    early(spread, 5)
+    spread(1, 3)
+    late(ring, 2)
+    ring(1, 6)
     early(spread, 6)
-    spread(1, 3)
+    late(ring, 3)
+    ring(1, 7)
+    late(ring, 4)
+    late(ring, 5)
+    upper(ring, 8)
+    late(ring, 6)
+    upper(ring, 9)
+    late(ring, 7)
     early(spread, 7)
-    ring(1, 5)
     early(spread, 8)
     spread(1, 4)
-
-    def to_last(t, _):
-        for side in (0, 1):
-            z_copy(1, t + 1, side, t).start()
-        return 0
-
-    @pl.when(z == 0)
-    def _():
-        pl.semaphore_wait(know.at[4], 1)
-        lax.fori_loop(0, 6, to_last, 0)
-
-    ring(1, 6)
-    pl.when(z == 0)(lambda: (to_last(6, 0), None)[1])
+    late(spread, 1)
     spread(1, 5)
-    late(ring, 1)
-    late(ring, 2)
+    late(spread, 2)
     spread(1, 6)
-    ring(1, 7)
-    late(spread, 1)
-    late(ring, 3)
-    late(spread, 2)
-    late(ring, 4)
+    late(spread, 3)
     spread(1, 7)
-    upper(ring, 8)
-    late(spread, 3)
-    late(ring, 5)
     late(spread, 4)
-    upper(ring, 9)
+    late(spread, 5)
     upper(spread, 8)
-    late(ring, 6)
-    late(spread, 5)
+    late(spread, 6)
     upper(spread, 9)
-    late(spread, 6)
+    late(spread, 7)
 
     for pos in range(2, 8):
         wv_copies[pos].wait()
@@ -637,7 +619,7 @@
         dma((2, 10)),
     ]
     scratch += [dma(())] * 6 + [dma((4,)), dma((4,)), dma(()), dma((8,)), dma(()), dma(())]
-    scratch += [pltpu.SemaphoreType.REGULAR((5,))]
+    scratch += [pltpu.SemaphoreType.REGULAR((3,))]
     spec = pl.BlockSpec(memory_space=pl.ANY)
     return pl.pallas_call(
         kernel,

time: 90 us -> 78.6 us (0.87)
  the two profiles are of different devices: /device:TPU:1825 before, /device:TPU:161 now
where the time goes in v3:
time: 78.6 us; the launch traced here: 78.5 us
  Pallas kernels  76.2 us (97%)
  local copies, waits for them, and re-layouts  2.3 us (3%)
    pallas_call x1, Pallas kernels, body(): pl.pallas_call(kernel, out_shape=jax.ShapeDtypeStruct((mine, width), BF16...  76.2 us
    unnamed x1, local copies, waits for them, and re-layouts  2.3 us

profile of v3, /device:TPU:161, one launch (start us, length us, event | category | flops | bytes accessed | tf_op | source)
XLA Modules:
  0.0 78.5 jit_solution(6523235267716432870)
XLA Ops:
  0.0 76.2 %gated_recurrence.1 = bf16[256,2048]{1,0:T(8,128)(2,1)} custom-call(bf16[2048,2048]{1,0:T(8,128)(2,1)} %tokens_in.1, f32[16,128]{1,0:T(8,128)} %bitcast.8, bf16[2048,256]{1,0:T(8,128)(2,1)} %w_input_in.1, bf16[2048,256]{1,0:T(8,128)(2,1)} %w_gate_in.1, f32[4,256]{1,0:T(4,128)} %taps_in.1, bf16[256,256]{1,0:T(8,128)(2,1)} %bitcast.6, ...), custom_call_target="tpu_custom_call" | custom-call | tf_op jit(solution)/shard_map/gated_recurrence/pallas_call | solution.py:624
  76.2 2.3 %copy.13 = bf16[256,2048]{1,0:T(8,128)(2,1)} copy(bf16[256,2048]{1,0:T(8,128)(2,1)} %gated_recurrence.1) | data formatting | bytes 2097152

commit v4 on v3

--- a/solution.py
+++ b/solution.py
@@ -129,7 +129,7 @@
         local(w_out_in.at[:, pl.ds(column(pos), channels)], wv.at[pos, own_lines, :], wv_sem.at[pos])
         for pos in range(8)
     ]
-    for pos in range(2):
+    for pos in range(4):
         wv_copies[pos].start()
     in_copies = [
         local(gain_in, gain, in_sem.at[0]),
@@ -153,7 +153,7 @@
         tok_copy(k).start()
     for k in range(3, 9):
         in_copies[k].start()
-    for pos in range(2, 8):
+    for pos in range(4, 8):
         wv_copies[pos].start()
 
     last = spans - 1
@@ -164,7 +164,6 @@
         + [{"tp": lax.rem(tp + k, peers)} for k in range(1, 8)]
     ):
         pl.semaphore_signal(barrier, inc=1, device_id=where, device_id_type=MESH)
-    pl.semaphore_wait(barrier, 10)
 
     def learn(level):
         pl.when(z < last)(lambda: pl.semaphore_wait(know.at[level], 1))
@@ -174,8 +173,6 @@
         def _():
             pl.semaphore_signal(know.at[level], inc=1, device_id={"sp": below}, device_id_type=MESH)
 
-    teach(0)
-
     place = below
 
     def from_below(span):
@@ -185,7 +182,7 @@
         return 9 - jnp.minimum(lax.rem(span + last, spans), 2)
 
     def z_copy(way, t, side, owner):
-        part = wv.at[side, lines_of(owner), :]
+        part = wv.at[2 * side : 2 * side + 2, lines_of(owner), :]
         where = {"sp": above if way == 0 else below}
         return remote(part, part, zs.at[way, t, side], zr.at[way, t, side], where)
 
@@ -194,15 +191,17 @@
 
     def share_copy(k, way, t):
         lines = lines_of(owner_of(way, t))
-        part = wv.at[0:2, lines, :]
         if k == 0:
             where = {"tp": lax.rem(tp + 2, peers)}
-            return remote(part, wv.at[6:8, lines, :], xs, xr.at[0, way, t], where)
+            return remote(wv.at[1, lines, :], wv.at[7, lines, :], xs, xr.at[0, way, t], where)
         if k == 1:
             where = {"tp": lax.rem(tp + 6, peers)}
-            return remote(part, wv.at[2:4, lines, :], xs, xr.at[1, way, t], where)
+            return remote(wv.at[2, lines, :], wv.at[4, lines, :], xs, xr.at[1, way, t], where)
         if k == 2:
-            return remote(part, wv.at[4:6, lines, :], ys, yr.at[way, t], {"grp": partner})
+            return remote(
+                wv.at[1:3, lines, :], wv.at[5:7, lines, :], ys, yr.at[way, t], {"grp": partner}
+            )
+        part = wv.at[0:4, lines, :]
         return remote(part, part, ds_send, ds_recv, {"tp": sibling})
 
     def ring(way, t):
@@ -221,21 +220,17 @@
     def spread(way, t):
         for k in range(3):
             share_copy(k, way, t).wait_recv()
-        part = wv.at[2:8, lines_of(owner_of(way, t)), :]
+        part = wv.at[4:8, lines_of(owner_of(way, t)), :]
         remote(part, part, ds_send, ds_recv, {"tp": sibling}).start()
 
     def early(act, t):
-        pl.when(place > t)(lambda: act(0, t))
-
-    for pos in range(2):
-        wv_copies[pos].wait()
+        step = t - jnp.where(z > 0, 0, 1)
+        pl.when(jnp.logical_and(place > t, step > 0))(lambda: act(0, step))
 
     def first_sends(way):
         for side in (0, 1):
             z_copy(way, 1, side, z).start()
 
-    first_sends(0)
-    first_sends(1)
 
     in_copies[0].wait()
     in_copies[1].wait()
@@ -271,17 +266,21 @@
                 scaled = acc[j * 64 : (j + 1) * 64, lane] * inv
                 proj[pl.ds(base + 8 + j * 64, 64), lane] = scaled.astype(BF16).astype(F32)
 
-        @pl.when(jnp.logical_and(i == 0, z < last))
-        def _():
-            halo_copy().start()
-
         return 0
 
-    lax.fori_loop(0, 2, project, 0)
+    lax.fori_loop(0, 1, project, 0)
+    pl.semaphore_wait(barrier, 10)
+    pl.when(z < last)(lambda: halo_copy().start())
+    teach(0)
+    for pos in range(4):
+        wv_copies[pos].wait()
+    first_sends(0)
+    first_sends(1)
+    lax.fori_loop(1, 3, project, 0)
     learn(0)
     teach(1)
     early(ring, 1)
-    lax.fori_loop(2, 4, project, 0)
+    lax.fori_loop(3, 4, project, 0)
     learn(1)
     teach(2)
     ring(1, 1)
@@ -379,6 +378,16 @@
     for k in (1, 2, 3):
         pl.when(z + k < spans)(lambda: carry_copy(k).start())
 
+    def state_copy():
+        return remote(
+            state_own, carry.at[3], carry_send.at[3], carry_recv.at[3], {"sp": lax.rem(z + 4, spans)}
+        )
+
+    @pl.when(z == 0)
+    def _():
+        state_own[...] = carry_own[...]
+        state_copy().start()
+
     in_copies[8].wait()
     for j in range(width // LANES):
         part = pl.ds(j * LANES, LANES)
@@ -403,10 +412,26 @@
     spread(1, 2)
     early(spread, 4)
 
-    def state_copy():
-        return remote(
-            state_own, carry.at[3], carry_send.at[3], carry_recv.at[3], {"sp": lax.rem(z + 4, spans)}
-        )
+    done = jnp.clip(place - 1, 0, jnp.where(z > 0, 8, 7))
+
+    def late(act, k):
+        pl.when(done + k <= from_below(z))(lambda: act(0, done + k))
+
+    def upper(act, t):
+        pl.when(t <= from_above(z))(lambda: act(1, t))
+
+    def services():
+        early(ring, 7)
+        early(ring, 8)
+        ring(1, 4)
+        early(spread, 5)
+        spread(1, 3)
+        late(ring, 1)
+        early(spread, 6)
+        ring(1, 5)
+        early(spread, 7)
+
+    pl.when(z > 0)(services)
 
     def received(copy, slot, k):
         pl.when(z >= k)(lambda: copy.wait_recv())
@@ -418,16 +443,21 @@
     received(state_copy(), 3, 4)
     for k in (1, 2, 3):
         received(carry_copy(k), k - 1, k)
-    incoming = []
+    incoming, out_states = [], []
     for c in range(lanes2):
         h = carry[3, lanes2 + c : lanes2 + c + 1, :]
         for k in (3, 2, 1):
             h = carry[k - 1, c : c + 1, :] * h + carry[k - 1, lanes2 + c : lanes2 + c + 1, :]
         incoming.append(h)
         out_state = carry_own[c : c + 1, :] * h + carry_own[lanes2 + c : lanes2 + c + 1, :]
-        state_own[c : c + 1, :] = jnp.zeros((1, LANES), F32)
-        state_own[lanes2 + c : lanes2 + c + 1, :] = out_state
-    pl.when(z + 4 < spans)(lambda: state_copy().start())
+        out_states.append(out_state)
+
+    @pl.when(jnp.logical_and(z > 0, z + 4 < spans))
+    def _():
+        for c in range(lanes2):
+            state_own[c : c + 1, :] = jnp.zeros((1, LANES), F32)
+            state_own[lanes2 + c : lanes2 + c + 1, :] = out_states[c]
+        state_copy().start()
 
     def a2a_copy(other):
         return remote(gout.at[other], grecv.at[tp], a2a_send, a2a_recv.at[tp], {"tp": other})
@@ -465,24 +495,9 @@
     grecv[tp] = gout[tp]
     ss_recv[tp] = ss_own[tp]
 
-    done = jnp.clip(place - 1, 0, 8)
-
-    def late(act, k):
-        pl.when(done + k <= from_below(z))(lambda: act(0, done + k))
-
-    def upper(act, t):
-        pl.when(t <= from_above(z))(lambda: act(1, t))
-
-    early(ring, 7)
-    early(ring, 8)
-    ring(1, 4)
-    late(ring, 1)
-    ring(1, 5)
-    early(spread, 5)
-    spread(1, 3)
+    pl.when(z == 0)(services)
     late(ring, 2)
     ring(1, 6)
-    early(spread, 6)
     late(ring, 3)
     ring(1, 7)
     late(ring, 4)
@@ -491,7 +506,6 @@
     late(ring, 6)
     upper(ring, 9)
     late(ring, 7)
-    early(spread, 7)
     early(spread, 8)
     spread(1, 4)
     late(spread, 1)
@@ -507,7 +521,7 @@
     upper(spread, 9)
     late(spread, 7)
 
-    for pos in range(2, 8):
+    for pos in range(4, 8):
         wv_copies[pos].wait()
     for k in range(1, 8):
         other = lax.rem(tp + k, peers)
@@ -537,10 +551,6 @@
     def out_copy(pos):
         return local(obuf.at[pos], out.at[:, pl.ds(column(pos), channels)], out_sem.at[pos])
 
-    for pos in range(8):
-        finish(pos, 0)
-        out_copy(pos).start()
-
     for way in (0, 1):
         count = from_below(above) if way == 0 else from_above(below)
 
@@ -550,9 +560,8 @@
             return 0
 
         lax.fori_loop(0, count, sent, 0)
-    shared = wv.at[0:4, pl.ds(0, 15 * share), :]
+    shared = wv.at[0:2, pl.ds(0, 15 * share), :]
     local(shared, shared, xs).wait()
-    shared = wv.at[0:2, pl.ds(0, 15 * share), :]
     local(shared, shared, ys).wait()
     local(everything, everything, ds_send).wait()
     pl.when(z < last)(lambda: halo_copy().wait_send())
@@ -563,6 +572,11 @@
     local(sent, sent, a2a_send).wait()
     sent = ss_own.at[pl.ds(0, 7)]
     local(sent, sent, ss_send).wait()
+    for pos in range(0, 8, 2):
+        finish(pos, 0)
+        finish(pos + 1, 0)
+        out_copy(pos).start()
+        out_copy(pos + 1).start()
     for pos in range(8):
         out_copy(pos).wait()
 

time: 78.6 us -> 74.8 us (0.952)
  the two profiles are of different devices: /device:TPU:161 before, /device:TPU:33 now
where the time goes in v4:
time: 74.8 us; the launch traced here: 73.6 us
  Pallas kernels  71.2 us (95%)
  local copies, waits for them, and re-layouts  2.3 us (3%)
    pallas_call x1, Pallas kernels, body(): pl.pallas_call(kernel, out_shape=jax.ShapeDtypeStruct((mine, width), BF16...  71.2 us
    unnamed x1, local copies, waits for them, and re-layouts  2.3 us

profile of v4, /device:TPU:33, one launch (start us, length us, event | category | flops | bytes accessed | tf_op | source)
XLA Modules:
  0.0 73.6 jit_solution(1317126297877311682)
XLA Ops:
  0.0 71.2 %gated_recurrence.1 = bf16[256,2048]{1,0:T(8,128)(2,1)} custom-call(bf16[2048,2048]{1,0:T(8,128)(2,1)} %tokens_in.1, f32[16,128]{1,0:T(8,128)} %bitcast.8, bf16[2048,256]{1,0:T(8,128)(2,1)} %w_input_in.1, bf16[2048,256]{1,0:T(8,128)(2,1)} %w_gate_in.1, f32[4,256]{1,0:T(4,128)} %taps_in.1, bf16[256,256]{1,0:T(8,128)(2,1)} %bitcast.6, ...), custom_call_target="tpu_custom_call" | custom-call | tf_op jit(solution)/shard_map/gated_recurrence/pallas_call | solution.py:638
  71.3 2.3 %copy.13 = bf16[256,2048]{1,0:T(8,128)(2,1)} copy(bf16[256,2048]{1,0:T(8,128)(2,1)} %gated_recurrence.1) | data formatting | bytes 2097152

commit v5 on v4

--- a/solution.py
+++ b/solution.py
@@ -103,7 +103,6 @@
     channels = wi.shape[1]
     lanes2 = channels // LANES
     block = width // spans
-    share = block // 2
     tile = rows // 4
     mine = rows // peers
     first = lax.rem(2 * (tp // 2) + 4 * lax.rem(grp, 2), 8)
@@ -120,9 +119,6 @@
         return pltpu.make_async_remote_copy(
             src_ref=src, dst_ref=dst, send_sem=send, recv_sem=recv, device_id=where, device_id_type=MESH
         )
-
-    def lines_of(owner):
-        return pl.ds(pl.multiple_of(owner * block + core * share, share), share)
 
     own_lines = pl.ds(pl.multiple_of(z * block, block), block)
     wv_copies = [
@@ -173,64 +169,66 @@
         def _():
             pl.semaphore_signal(know.at[level], inc=1, device_id={"sp": below}, device_id_type=MESH)
 
-    place = below
-
-    def from_below(span):
-        return jnp.minimum(lax.rem(span + last, spans), 2) + 6
-
-    def from_above(span):
-        return 9 - jnp.minimum(lax.rem(span + last, spans), 2)
-
-    def z_copy(way, t, side, owner):
-        part = wv.at[2 * side : 2 * side + 2, lines_of(owner), :]
-        where = {"sp": above if way == 0 else below}
-        return remote(part, part, zs.at[way, t, side], zr.at[way, t, side], where)
+    low = jnp.minimum(below, 2)
+    count = (1 - core) * (low + 6) + core * (9 - low)
+    onward = lax.rem(z + 1 + core * (spans - 2), spans)
+    low = jnp.minimum(lax.rem(onward + last, spans), 2)
+    count_out = (1 - core) * (low + 6) + core * (9 - low)
+    count_other = spans - 1 - count
 
     def owner_of(way, t):
-        return lax.rem(z + spans - t, spans) if way == 0 else lax.rem(z + t, spans)
-
-    def share_copy(k, way, t):
-        lines = lines_of(owner_of(way, t))
-        if k == 0:
-            where = {"tp": lax.rem(tp + 2, peers)}
-            return remote(wv.at[1, lines, :], wv.at[7, lines, :], xs, xr.at[0, way, t], where)
-        if k == 1:
-            where = {"tp": lax.rem(tp + 6, peers)}
-            return remote(wv.at[2, lines, :], wv.at[4, lines, :], xs, xr.at[1, way, t], where)
-        if k == 2:
+        return lax.rem(z + (1 - way) * (spans - t) + way * t, spans)
+
+    def lines_of(owner):
+        return pl.ds(pl.multiple_of(owner * block, block), block)
+
+    def z_copy(t, pos, owner):
+        part = wv.at[pos, lines_of(owner), :]
+        return remote(part, part, zs.at[t, pos], zr.at[t, pos], {"sp": onward})
+
+    def share_copy(k, t):
+        lines = lines_of(owner_of(core, t))
+        if k < 2:
+            where = {"tp": lax.rem(tp + 2 + 4 * k, peers)}
             return remote(
-                wv.at[1:3, lines, :], wv.at[5:7, lines, :], ys, yr.at[way, t], {"grp": partner}
+                wv.at[1 + k, lines, :], wv.at[7 - 3 * k, lines, :], xs.at[k, t], xr.at[k, t], where
             )
-        part = wv.at[0:4, lines, :]
-        return remote(part, part, ds_send, ds_recv, {"tp": sibling})
-
-    def ring(way, t):
-        owner = owner_of(way, t)
-        more = t + 1 <= (from_below(above) if way == 0 else from_above(below))
-        for side in (0, 1):
-            z_copy(way, t, side, owner).wait_recv()
-
-            @pl.when(more)
+        return remote(
+            wv.at[1:3, lines, :], wv.at[5:7, lines, :], ys.at[t], yr.at[t], {"grp": partner}
+        )
+
+    def d_copy(level, way, t):
+        part = wv.at[4 * level : 4 * level + 4, lines_of(owner_of(way, t)), :]
+        return remote(part, part, ds_send.at[level, t], ds_recv.at[level, t], {"tp": sibling})
+
+    def ring(t, _):
+        owner = owner_of(core, t)
+        for pos in (1, 2, 0, 3):
+            z_copy(t, pos, owner).wait_recv()
+
+            @pl.when(t < count_out)
             def _():
-                z_copy(way, t + 1, side, owner).start()
-
-        for k in range(4):
-            share_copy(k, way, t).start()
-
-    def spread(way, t):
+                z_copy(t + 1, pos, owner).start()
+
         for k in range(3):
-            share_copy(k, way, t).wait_recv()
-        part = wv.at[4:8, lines_of(owner_of(way, t)), :]
-        remote(part, part, ds_send, ds_recv, {"tp": sibling}).start()
-
-    def early(act, t):
-        step = t - jnp.where(z > 0, 0, 1)
-        pl.when(jnp.logical_and(place > t, step > 0))(lambda: act(0, step))
-
-    def first_sends(way):
-        for side in (0, 1):
-            z_copy(way, 1, side, z).start()
-
+            share_copy(k, t).start()
+        d_copy(0, core, t).start()
+        return 0
+
+    def spread(t, _):
+        for k in range(3):
+            share_copy(k, t).wait_recv()
+        d_copy(1, core, t).start()
+        return 0
+
+    def goal(up, down, at_first):
+        up = jnp.minimum(up, jnp.maximum(below - 1, 0))
+        up = jnp.where(z > 0, up, at_first)
+        return (1 - core) * up + core * down
+
+    def first_sends():
+        for pos in (1, 2, 0, 3):
+            z_copy(1, pos, z).start()
 
     in_copies[0].wait()
     in_copies[1].wait()
@@ -274,17 +272,15 @@
     teach(0)
     for pos in range(4):
         wv_copies[pos].wait()
-    first_sends(0)
-    first_sends(1)
+    first_sends()
     lax.fori_loop(1, 3, project, 0)
+    r0 = goal(1, 0, 0)
+    lax.fori_loop(1, r0 + 1, ring, 0)
+    lax.fori_loop(3, 4, project, 0)
     learn(0)
     teach(1)
-    early(ring, 1)
-    lax.fori_loop(3, 4, project, 0)
-    learn(1)
-    teach(2)
-    ring(1, 1)
-    early(ring, 2)
+    r1 = goal(2, 0, 0)
+    lax.fori_loop(r0 + 1, r1 + 1, ring, 0)
 
     for k in range(3, 8):
         in_copies[k].wait()
@@ -348,12 +344,13 @@
 
     state = (jnp.zeros((SEGS, LANES), F32), jnp.ones((SEGS, LANES), F32)) * lanes2
     state = lax.fori_loop(0, 3, scan_tile, state)
-    early(ring, 3)
+    learn(1)
+    teach(2)
+    r2 = goal(3, 1, 0)
+    lax.fori_loop(r1 + 1, r2 + 1, ring, 0)
     state = lax.fori_loop(3, 6, scan_tile, state)
-    ring(1, 2)
-    early(ring, 4)
-    early(spread, 1)
-    spread(1, 1)
+    r3 = goal(4, 1, 0)
+    lax.fori_loop(r2 + 1, r3 + 1, ring, 0)
     state = lax.fori_loop(6, 8, scan_tile, state)
 
     for c in range(lanes2):
@@ -388,6 +385,11 @@
         state_own[...] = carry_own[...]
         state_copy().start()
 
+    r4 = goal(5, 2, 1)
+    lax.fori_loop(r3 + 1, r4 + 1, ring, 0)
+    s0 = goal(2, 0, 0)
+    lax.fori_loop(1, s0 + 1, spread, 0)
+
     in_copies[8].wait()
     for j in range(width // LANES):
         part = pl.ds(j * LANES, LANES)
@@ -403,35 +405,18 @@
         return 0
 
     lax.fori_loop(0, 2, gate, 0)
-    early(ring, 5)
-    early(spread, 2)
-    early(spread, 3)
+    r5 = goal(6, 2, 1)
+    lax.fori_loop(r4 + 1, r5 + 1, ring, 0)
     lax.fori_loop(2, 4, gate, 0)
-    ring(1, 3)
-    early(ring, 6)
-    spread(1, 2)
-    early(spread, 4)
-
-    done = jnp.clip(place - 1, 0, jnp.where(z > 0, 8, 7))
-
-    def late(act, k):
-        pl.when(done + k <= from_below(z))(lambda: act(0, done + k))
-
-    def upper(act, t):
-        pl.when(t <= from_above(z))(lambda: act(1, t))
-
-    def services():
-        early(ring, 7)
-        early(ring, 8)
-        ring(1, 4)
-        early(spread, 5)
-        spread(1, 3)
-        late(ring, 1)
-        early(spread, 6)
-        ring(1, 5)
-        early(spread, 7)
-
-    pl.when(z > 0)(services)
+    r6 = goal(7, 3, 3)
+    lax.fori_loop(r5 + 1, r6 + 1, ring, 0)
+    s1 = goal(4, 1, 0)
+    lax.fori_loop(s0 + 1, s1 + 1, spread, 0)
+
+    r7 = jnp.where(z > 0, (1 - core) * jnp.minimum(z, 8) + core * 6, r6)
+    lax.fori_loop(r6 + 1, r7 + 1, ring, 0)
+    s2 = jnp.where(z > 0, goal(7, 4, 0), s1)
+    lax.fori_loop(s1 + 1, s2 + 1, spread, 0)
 
     def received(copy, slot, k):
         pl.when(z >= k)(lambda: copy.wait_recv())
@@ -495,31 +480,8 @@
     grecv[tp] = gout[tp]
     ss_recv[tp] = ss_own[tp]
 
-    pl.when(z == 0)(services)
-    late(ring, 2)
-    ring(1, 6)
-    late(ring, 3)
-    ring(1, 7)
-    late(ring, 4)
-    late(ring, 5)
-    upper(ring, 8)
-    late(ring, 6)
-    upper(ring, 9)
-    late(ring, 7)
-    early(spread, 8)
-    spread(1, 4)
-    late(spread, 1)
-    spread(1, 5)
-    late(spread, 2)
-    spread(1, 6)
-    late(spread, 3)
-    spread(1, 7)
-    late(spread, 4)
-    late(spread, 5)
-    upper(spread, 8)
-    late(spread, 6)
-    upper(spread, 9)
-    late(spread, 7)
+    lax.fori_loop(r7 + 1, count + 1, ring, 0)
+    lax.fori_loop(s2 + 1, count + 1, spread, 0)
 
     for pos in range(4, 8):
         wv_copies[pos].wait()
@@ -528,8 +490,13 @@
         remote(gout.at[other], grecv.at[other], a2a_send, a2a_recv.at[other], {"tp": other}).wait_recv()
     seven = ss_recv.at[pl.ds(0, 7)]
     local(seven, seven, ss_recv_sem).wait()
-    everything = wv.at[:, pl.ds(0, 15 * share), :]
-    local(everything, everything, ds_recv).wait()
+
+    def other_half(t, _):
+        d_copy(0, 1 - core, t).wait_recv()
+        d_copy(1, 1 - core, t).wait_recv()
+        return 0
+
+    lax.fori_loop(1, count_other + 1, other_half, 0)
 
     total = ss_recv[0]
     for k in range(1, 8):
@@ -551,19 +518,20 @@
     def out_copy(pos):
         return local(obuf.at[pos], out.at[:, pl.ds(column(pos), channels)], out_sem.at[pos])
 
-    for way in (0, 1):
-        count = from_below(above) if way == 0 else from_above(below)
-
-        def sent(t, _):
-            for side in (0, 1):
-                z_copy(way, t + 1, side, z).wait_send()
-            return 0
-
-        lax.fori_loop(0, count, sent, 0)
-    shared = wv.at[0:2, pl.ds(0, 15 * share), :]
-    local(shared, shared, xs).wait()
-    local(shared, shared, ys).wait()
-    local(everything, everything, ds_send).wait()
+    def passed(t, _):
+        for pos in range(4):
+            z_copy(t, pos, z).wait_send()
+        return 0
+
+    def shared(t, _):
+        for k in range(3):
+            share_copy(k, t).wait_send()
+        d_copy(0, core, t).wait_send()
+        d_copy(1, core, t).wait_send()
+        return 0
+
+    lax.fori_loop(1, count_out + 1, passed, 0)
+    lax.fori_loop(1, count + 1, shared, 0)
     pl.when(z < last)(lambda: halo_copy().wait_send())
     for k in (1, 2, 3):
         pl.when(z + k < spans)(lambda: carry_copy(k).wait_send())
@@ -627,12 +595,23 @@
         dma((9,)),
         dma((8,)),
         dma((8,)),
-        dma((2, 10, 2)),
-        dma((2, 10, 2)),
-        dma((2, 2, 10)),
+        dma((10, 4)),
+        dma((10, 4)),
         dma((2, 10)),
+        dma((10,)),
+        dma((2, 10)),
+        dma((10,)),
+        dma((2, 10)),
+        dma((2, 10)),
+        dma(()),
+        dma(()),
+        dma((4,)),
+        dma((4,)),
+        dma(()),
+        dma((8,)),
+        dma(()),
+        dma(()),
     ]
-    scratch += [dma(())] * 6 + [dma((4,)), dma((4,)), dma(()), dma((8,)), dma(()), dma(())]
     scratch += [pltpu.SemaphoreType.REGULAR((3,))]
     spec = pl.BlockSpec(memory_space=pl.ANY)
     return pl.pallas_call(

time: 74.8 us -> 67.9 us (0.908); the launches traced: 73.6 us -> 67.8 us
  Pallas kernels: 71.2 us -> 65.5 us
    pallas_call x1, Pallas kernels: 71.2 us -> 65.5 us  [body(): pl.pallas_call(kernel, out_shape=jax.ShapeDtypeStruct((mine, width), BF16...]
where the time goes in v5:
time: 67.9 us; the launch traced here: 67.8 us
  Pallas kernels  65.5 us (96%)
  local copies, waits for them, and re-layouts  2.3 us (3%)
    pallas_call x1, Pallas kernels, body(): pl.pallas_call(kernel, out_shape=jax.ShapeDtypeStruct((mine, width), BF16...  65.5 us
    unnamed x1, local copies, waits for them, and re-layouts  2.3 us

profile of v5, /device:TPU:33, one launch (start us, length us, event | category | flops | bytes accessed | tf_op | source)
XLA Modules:
  0.0 67.8 jit_solution(372472596779237433)
XLA Ops:
  0.0 65.5 %gated_recurrence.1 = bf16[256,2048]{1,0:T(8,128)(2,1)} custom-call(bf16[2048,2048]{1,0:T(8,128)(2,1)} %tokens_in.1, f32[16,128]{1,0:T(8,128)} %bitcast.8, bf16[2048,256]{1,0:T(8,128)(2,1)} %w_input_in.1, bf16[2048,256]{1,0:T(8,128)(2,1)} %w_gate_in.1, f32[4,256]{1,0:T(4,128)} %taps_in.1, bf16[256,256]{1,0:T(8,128)(2,1)} %bitcast.6, ...), custom_call_target="tpu_custom_call" | custom-call | tf_op jit(solution)/shard_map/gated_recurrence/pallas_call | solution.py:617
  65.5 2.3 %copy.13 = bf16[256,2048]{1,0:T(8,128)(2,1)} copy(bf16[256,2048]{1,0:T(8,128)(2,1)} %gated_recurrence.1) | data formatting | bytes 2097152

commit v6 on v5

--- a/solution.py
+++ b/solution.py
@@ -169,11 +169,13 @@
         def _():
             pl.semaphore_signal(know.at[level], inc=1, device_id={"sp": below}, device_id_type=MESH)
 
-    low = jnp.minimum(below, 2)
-    count = (1 - core) * (low + 6) + core * (9 - low)
+    def blocks_at(span):
+        low = jnp.minimum(lax.rem(span + last, spans), 3) + 5 - jnp.where(span > 0, 0, 1)
+        return (1 - core) * low + core * (spans - 1 - low)
+
+    count = blocks_at(z)
     onward = lax.rem(z + 1 + core * (spans - 2), spans)
-    low = jnp.minimum(lax.rem(onward + last, spans), 2)
-    count_out = (1 - core) * (low + 6) + core * (9 - low)
+    count_out = blocks_at(onward)
     count_other = spans - 1 - count
 
     def owner_of(way, t):
@@ -221,10 +223,9 @@
         d_copy(1, core, t).start()
         return 0
 
-    def goal(up, down, at_first):
-        up = jnp.minimum(up, jnp.maximum(below - 1, 0))
-        up = jnp.where(z > 0, up, at_first)
-        return (1 - core) * up + core * down
+    def goal(up, down, first_up, first_down):
+        up = jnp.where(z > 0, jnp.minimum(up, jnp.maximum(z - 2, 0)), first_up)
+        return (1 - core) * up + core * jnp.where(z > 0, down, first_down)
 
     def first_sends():
         for pos in (1, 2, 0, 3):
@@ -273,14 +274,9 @@
     for pos in range(4):
         wv_copies[pos].wait()
     first_sends()
-    lax.fori_loop(1, 3, project, 0)
-    r0 = goal(1, 0, 0)
-    lax.fori_loop(1, r0 + 1, ring, 0)
-    lax.fori_loop(3, 4, project, 0)
+    lax.fori_loop(1, 4, project, 0)
     learn(0)
     teach(1)
-    r1 = goal(2, 0, 0)
-    lax.fori_loop(r0 + 1, r1 + 1, ring, 0)
 
     for k in range(3, 8):
         in_copies[k].wait()
@@ -346,11 +342,11 @@
     state = lax.fori_loop(0, 3, scan_tile, state)
     learn(1)
     teach(2)
-    r2 = goal(3, 1, 0)
-    lax.fori_loop(r1 + 1, r2 + 1, ring, 0)
+    r0 = goal(1, 0, 0, 0)
+    lax.fori_loop(1, r0 + 1, ring, 0)
     state = lax.fori_loop(3, 6, scan_tile, state)
-    r3 = goal(4, 1, 0)
-    lax.fori_loop(r2 + 1, r3 + 1, ring, 0)
+    r1 = goal(1, 1, 0, 1)
+    lax.fori_loop(r0 + 1, r1 + 1, ring, 0)
     state = lax.fori_loop(6, 8, scan_tile, state)
 
     for c in range(lanes2):
@@ -385,10 +381,8 @@
         state_own[...] = carry_own[...]
         state_copy().start()
 
-    r4 = goal(5, 2, 1)
-    lax.fori_loop(r3 + 1, r4 + 1, ring, 0)
-    s0 = goal(2, 0, 0)
-    lax.fori_loop(1, s0 + 1, spread, 0)
+    r2 = goal(2, 1, 1, 2)
+    lax.fori_loop(r1 + 1, r2 + 1, ring, 0)
 
     in_copies[8].wait()
     for j in range(width // LANES):
@@ -404,19 +398,16 @@
             ge[part, lane] = gelu((acc[:, lane] * inv).astype(BF16).astype(F32))
         return 0
 
-    lax.fori_loop(0, 2, gate, 0)
-    r5 = goal(6, 2, 1)
-    lax.fori_loop(r4 + 1, r5 + 1, ring, 0)
-    lax.fori_loop(2, 4, gate, 0)
-    r6 = goal(7, 3, 3)
-    lax.fori_loop(r5 + 1, r6 + 1, ring, 0)
-    s1 = goal(4, 1, 0)
+    lax.fori_loop(0, 4, gate, 0)
+    r3 = goal(3, 2, 1, 3)
+    lax.fori_loop(r2 + 1, r3 + 1, ring, 0)
+    s0 = goal(1, 1, 0, 0)
+    lax.fori_loop(1, s0 + 1, spread, 0)
+
+    r4 = goal(8, 5, 1, 3)
+    lax.fori_loop(r3 + 1, r4 + 1, ring, 0)
+    s1 = goal(7, 4, 0, 0)
     lax.fori_loop(s0 + 1, s1 + 1, spread, 0)
-
-    r7 = jnp.where(z > 0, (1 - core) * jnp.minimum(z, 8) + core * 6, r6)
-    lax.fori_loop(r6 + 1, r7 + 1, ring, 0)
-    s2 = jnp.where(z > 0, goal(7, 4, 0), s1)
-    lax.fori_loop(s1 + 1, s2 + 1, spread, 0)
 
     def received(copy, slot, k):
         pl.when(z >= k)(lambda: copy.wait_recv())
@@ -464,8 +455,7 @@
             total = total + gated * gated
             gout[s, :, lane] = (gated * ogain[:, lane]).astype(BF16)
         sums = lax.dot_general(
-            ones, total, (((1,), (1,)), ((), ())), precision=lax.Precision.HIGHEST,
-            preferred_element_type=F32,
+            ones, total, (((1,), (1,)), ((), ())), preferred_element_type=F32
         )
         ss_own[s] = sums[0:1, :]
 
@@ -480,8 +470,8 @@
     grecv[tp] = gout[tp]
     ss_recv[tp] = ss_own[tp]
 
-    lax.fori_loop(r7 + 1, count + 1, ring, 0)
-    lax.fori_loop(s2 + 1, count + 1, spread, 0)
+    lax.fori_loop(r4 + 1, count + 1, ring, 0)
+    lax.fori_loop(s1 + 1, count + 1, spread, 0)
 
     for pos in range(4, 8):
         wv_copies[pos].wait()
@@ -540,11 +530,10 @@
     local(sent, sent, a2a_send).wait()
     sent = ss_own.at[pl.ds(0, 7)]
     local(sent, sent, ss_send).wait()
-    for pos in range(0, 8, 2):
+    for pos in range(8):
         finish(pos, 0)
-        finish(pos + 1, 0)
+    for pos in range(8):
         out_copy(pos).start()
-        out_copy(pos + 1).start()
     for pos in range(8):
         out_copy(pos).wait()
 
@@ -595,14 +584,14 @@
         dma((9,)),
         dma((8,)),
         dma((8,)),
-        dma((10, 4)),
-        dma((10, 4)),
-        dma((2, 10)),
-        dma((10,)),
-        dma((2, 10)),
-        dma((10,)),
-        dma((2, 10)),
-        dma((2, 10)),
+        dma((11, 4)),
+        dma((11, 4)),
+        dma((2, 11)),
+        dma((11,)),
+        dma((2, 11)),
+        dma((11,)),
+        dma((2, 11)),
+        dma((2, 11)),
         dma(()),
         dma(()),
         dma((4,)),

time: 67.9 us -> 70.5 us (1.038)
  the two profiles are of different devices: /device:TPU:33 before, /device:TPU:161 now
where the time goes in v6:
time: 70.5 us; the launch traced here: 70.4 us
  Pallas kernels  68.1 us (97%)
  local copies, waits for them, and re-layouts  2.3 us (3%)
    pallas_call x1, Pallas kernels, body(): pl.pallas_call(kernel, out_shape=jax.ShapeDtypeStruct((mine, width), BF16...  68.1 us
    unnamed x1, local copies, waits for them, and re-layouts  2.3 us

profile of v6, /device:TPU:161, one launch (start us, length us, event | category | flops | bytes accessed | tf_op | source)
XLA Modules:
  0.0 70.4 jit_solution(12835093728900585757)
XLA Ops:
  0.0 68.1 %gated_recurrence.1 = bf16[256,2048]{1,0:T(8,128)(2,1)} custom-call(bf16[2048,2048]{1,0:T(8,128)(2,1)} %tokens_in.1, f32[16,128]{1,0:T(8,128)} %bitcast.8, bf16[2048,256]{1,0:T(8,128)(2,1)} %w_input_in.1, bf16[2048,256]{1,0:T(8,128)(2,1)} %w_gate_in.1, f32[4,256]{1,0:T(4,128)} %taps_in.1, bf16[256,256]{1,0:T(8,128)(2,1)} %bitcast.6, ...), custom_call_target="tpu_custom_call" | custom-call | tf_op jit(solution)/shard_map/gated_recurrence/pallas_call | solution.py:606
  68.1 2.3 %copy.13 = bf16[256,2048]{1,0:T(8,128)(2,1)} copy(bf16[256,2048]{1,0:T(8,128)(2,1)} %gated_recurrence.1) | data formatting | bytes 2097152

commit v7 on v6

--- a/solution.py
+++ b/solution.py
@@ -170,7 +170,7 @@
             pl.semaphore_signal(know.at[level], inc=1, device_id={"sp": below}, device_id_type=MESH)
 
     def blocks_at(span):
-        low = jnp.minimum(lax.rem(span + last, spans), 3) + 5 - jnp.where(span > 0, 0, 1)
+        low = jnp.minimum(lax.rem(span + last, spans), 2) + 6 - jnp.where(span > 0, 0, 2)
         return (1 - core) * low + core * (spans - 1 - low)
 
     count = blocks_at(z)
@@ -225,7 +225,8 @@
 
     def goal(up, down, first_up, first_down):
         up = jnp.where(z > 0, jnp.minimum(up, jnp.maximum(z - 2, 0)), first_up)
-        return (1 - core) * up + core * jnp.where(z > 0, down, first_down)
+        down = jnp.where(z > 0, jnp.where(z == 1, jnp.maximum(down, 4), down), first_down)
+        return (1 - core) * up + core * down
 
     def first_sends():
         for pos in (1, 2, 0, 3):
@@ -280,6 +281,8 @@
 
     for k in range(3, 8):
         in_copies[k].wait()
+    ahead = jnp.where(z == 1, 4 * core, 0)
+    lax.fori_loop(1, ahead + 1, ring, 0)
     pl.when(z > 0)(lambda: halo_copy().wait_recv())
 
     @pl.when(z > 0)
@@ -342,10 +345,10 @@
     state = lax.fori_loop(0, 3, scan_tile, state)
     learn(1)
     teach(2)
-    r0 = goal(1, 0, 0, 0)
-    lax.fori_loop(1, r0 + 1, ring, 0)
+    r0 = goal(1, 0, 0, 1)
+    lax.fori_loop(ahead + 1, r0 + 1, ring, 0)
     state = lax.fori_loop(3, 6, scan_tile, state)
-    r1 = goal(1, 1, 0, 1)
+    r1 = goal(1, 1, 0, 2)
     lax.fori_loop(r0 + 1, r1 + 1, ring, 0)
     state = lax.fori_loop(6, 8, scan_tile, state)
 
@@ -381,7 +384,7 @@
         state_own[...] = carry_own[...]
         state_copy().start()
 
-    r2 = goal(2, 1, 1, 2)
+    r2 = goal(1, 1, 1, 3)
     lax.fori_loop(r1 + 1, r2 + 1, ring, 0)
 
     in_copies[8].wait()
@@ -398,15 +401,18 @@
             ge[part, lane] = gelu((acc[:, lane] * inv).astype(BF16).astype(F32))
         return 0
 
-    lax.fori_loop(0, 4, gate, 0)
-    r3 = goal(3, 2, 1, 3)
-    lax.fori_loop(r2 + 1, r3 + 1, ring, 0)
-    s0 = goal(1, 1, 0, 0)
+    lax.fori_loop(0, 2, gate, 0)
+    rg = goal(2, 1, 1, 4)
+    lax.fori_loop(r2 + 1, rg + 1, ring, 0)
+    lax.fori_loop(2, 4, gate, 0)
+    r3 = goal(3, 2, 1, 5)
+    lax.fori_loop(rg + 1, r3 + 1, ring, 0)
+    s0 = goal(1, 1, 0, 2)
     lax.fori_loop(1, s0 + 1, spread, 0)
 
-    r4 = goal(8, 5, 1, 3)
+    r4 = goal(8, 5, 1, 5)
     lax.fori_loop(r3 + 1, r4 + 1, ring, 0)
-    s1 = goal(7, 4, 0, 0)
+    s1 = goal(7, 4, 0, 2)
     lax.fori_loop(s0 + 1, s1 + 1, spread, 0)
 
     def received(copy, slot, k):
@@ -470,8 +476,13 @@
     grecv[tp] = gout[tp]
     ss_recv[tp] = ss_own[tp]
 
-    lax.fori_loop(r4 + 1, count + 1, ring, 0)
-    lax.fori_loop(s1 + 1, count + 1, spread, 0)
+    def both(t, _):
+        ring(t, 0)
+        pl.when(t - 3 > s1)(lambda: (spread(t - 3, 0), None)[1])
+        return 0
+
+    lax.fori_loop(r4 + 1, count + 1, both, 0)
+    lax.fori_loop(jnp.maximum(s1, jnp.where(count > r4, count - 3, s1)) + 1, count + 1, spread, 0)
 
     for pos in range(4, 8):
         wv_copies[pos].wait()
@@ -502,11 +513,13 @@
             )
         for c in range(lanes2):
             lane = slice(c * LANES, (c + 1) * LANES)
-            obuf[pos, :, lane] = (acc[:, lane] * scales).astype(BF16)
-        return 0
-
-    def out_copy(pos):
-        return local(obuf.at[pos], out.at[:, pl.ds(column(pos), channels)], out_sem.at[pos])
+            where = pl.ds(pl.multiple_of(column(pos) + c * LANES, LANES), LANES)
+            obuf[:, where] = (acc[:, lane] * scales).astype(BF16)
+        return 0
+
+    def out_copy(k):
+        part = pl.ds(k * (mine // 4), mine // 4)
+        return local(obuf.at[part, :], out.at[part, :], out_sem.at[k])
 
     def passed(t, _):
         for pos in range(4):
@@ -532,10 +545,10 @@
     local(sent, sent, ss_send).wait()
     for pos in range(8):
         finish(pos, 0)
-    for pos in range(8):
-        out_copy(pos).start()
-    for pos in range(8):
-        out_copy(pos).wait()
+    for k in range(4):
+        out_copy(k).start()
+    for k in range(4):
+        out_copy(k).wait()
 
 
 def body(
@@ -579,7 +592,7 @@
         vmem((peers, mine, channels), BF16),
         vmem((peers, 1, mine), F32),
         vmem((peers, 1, mine), F32),
-        vmem((8, mine, channels), BF16),
+        vmem((mine, width), BF16),
         dma((4,)),
         dma((9,)),
         dma((8,)),

time: 70.5 us -> 71.2 us (level)
  the two profiles are of different devices: /device:TPU:161 before, /device:TPU:417 now
where the time goes in v7:
time: 71.2 us; the launch traced here: 71 us
  Pallas kernels  68.7 us (96%)
  local copies, waits for them, and re-layouts  2.3 us (3%)
    pallas_call x1, Pallas kernels, body(): pl.pallas_call(kernel, out_shape=jax.ShapeDtypeStruct((mine, width), BF16...  68.7 us
    unnamed x1, local copies, waits for them, and re-layouts  2.3 us

profile of v7, /device:TPU:417, one launch (start us, length us, event | category | flops | bytes accessed | tf_op | source)
XLA Modules:
  0.0 71.0 jit_solution(7932507382078719147)
XLA Ops:
  0.0 68.7 %gated_recurrence.1 = bf16[256,2048]{1,0:T(8,128)(2,1)} custom-call(bf16[2048,2048]{1,0:T(8,128)(2,1)} %tokens_in.1, f32[16,128]{1,0:T(8,128)} %bitcast.8, bf16[2048,256]{1,0:T(8,128)(2,1)} %w_input_in.1, bf16[2048,256]{1,0:T(8,128)(2,1)} %w_gate_in.1, f32[4,256]{1,0:T(4,128)} %taps_in.1, bf16[256,256]{1,0:T(8,128)(2,1)} %bitcast.6, ...), custom_call_target="tpu_custom_call" | custom-call | tf_op jit(solution)/shard_map/gated_recurrence/pallas_call | solution.py:619
  68.7 2.3 %copy.13 = bf16[256,2048]{1,0:T(8,128)(2,1)} copy(bf16[256,2048]{1,0:T(8,128)(2,1)} %gated_recurrence.1) | data formatting | bytes 2097152

commit v8 on v7

--- a/solution.py
+++ b/solution.py
@@ -170,7 +170,7 @@
             pl.semaphore_signal(know.at[level], inc=1, device_id={"sp": below}, device_id_type=MESH)
 
     def blocks_at(span):
-        low = jnp.minimum(lax.rem(span + last, spans), 2) + 6 - jnp.where(span > 0, 0, 2)
+        low = jnp.minimum(lax.rem(span + last, spans), 2) + 6 - jnp.where(span > 0, 0, 1)
         return (1 - core) * low + core * (spans - 1 - low)
 
     count = blocks_at(z)
@@ -225,7 +225,7 @@
 
     def goal(up, down, first_up, first_down):
         up = jnp.where(z > 0, jnp.minimum(up, jnp.maximum(z - 2, 0)), first_up)
-        down = jnp.where(z > 0, jnp.where(z == 1, jnp.maximum(down, 4), down), first_down)
+        down = jnp.where(z > 0, jnp.where(z == 1, jnp.maximum(down, 3), down), first_down)
         return (1 - core) * up + core * down
 
     def first_sends():
@@ -275,14 +275,19 @@
     for pos in range(4):
         wv_copies[pos].wait()
     first_sends()
-    lax.fori_loop(1, 4, project, 0)
+    lax.fori_loop(1, 3, project, 0)
+    rp = (1 - core) * jnp.where(z > 0, jnp.clip(z - 2, 0, 1), 0)
+    lax.fori_loop(1, rp + 1, ring, 0)
+    lax.fori_loop(3, 4, project, 0)
     learn(0)
     teach(1)
+    ra = (1 - core) * jnp.where(z > 0, jnp.clip(z - 2, 0, 2), 0)
+    lax.fori_loop(rp + 1, ra + 1, ring, 0)
 
     for k in range(3, 8):
         in_copies[k].wait()
-    ahead = jnp.where(z == 1, 4 * core, 0)
-    lax.fori_loop(1, ahead + 1, ring, 0)
+    ahead = jnp.where(z == 1, 3 * core, ra)
+    lax.fori_loop(ra + 1, ahead + 1, ring, 0)
     pl.when(z > 0)(lambda: halo_copy().wait_recv())
 
     @pl.when(z > 0)
@@ -345,10 +350,10 @@
     state = lax.fori_loop(0, 3, scan_tile, state)
     learn(1)
     teach(2)
-    r0 = goal(1, 0, 0, 1)
+    r0 = goal(3, 1, 0, 1)
     lax.fori_loop(ahead + 1, r0 + 1, ring, 0)
     state = lax.fori_loop(3, 6, scan_tile, state)
-    r1 = goal(1, 1, 0, 2)
+    r1 = goal(4, 1, 0, 2)
     lax.fori_loop(r0 + 1, r1 + 1, ring, 0)
     state = lax.fori_loop(6, 8, scan_tile, state)
 
@@ -384,7 +389,7 @@
         state_own[...] = carry_own[...]
         state_copy().start()
 
-    r2 = goal(1, 1, 1, 3)
+    r2 = goal(5, 2, 1, 3)
     lax.fori_loop(r1 + 1, r2 + 1, ring, 0)
 
     in_copies[8].wait()
@@ -402,15 +407,15 @@
         return 0
 
     lax.fori_loop(0, 2, gate, 0)
-    rg = goal(2, 1, 1, 4)
+    rg = goal(6, 2, 1, 4)
     lax.fori_loop(r2 + 1, rg + 1, ring, 0)
     lax.fori_loop(2, 4, gate, 0)
-    r3 = goal(3, 2, 1, 5)
+    r3 = goal(7, 3, 2, 5)
     lax.fori_loop(rg + 1, r3 + 1, ring, 0)
-    s0 = goal(1, 1, 0, 2)
+    s0 = goal(4, 1, 0, 2)
     lax.fori_loop(1, s0 + 1, spread, 0)
 
-    r4 = goal(8, 5, 1, 5)
+    r4 = goal(8, 5, 2, 5)
     lax.fori_loop(r3 + 1, r4 + 1, ring, 0)
     s1 = goal(7, 4, 0, 2)
     lax.fori_loop(s0 + 1, s1 + 1, spread, 0)
@@ -476,13 +481,8 @@
     grecv[tp] = gout[tp]
     ss_recv[tp] = ss_own[tp]
 
-    def both(t, _):
-        ring(t, 0)
-        pl.when(t - 3 > s1)(lambda: (spread(t - 3, 0), None)[1])
-        return 0
-
-    lax.fori_loop(r4 + 1, count + 1, both, 0)
-    lax.fori_loop(jnp.maximum(s1, jnp.where(count > r4, count - 3, s1)) + 1, count + 1, spread, 0)
+    lax.fori_loop(r4 + 1, count + 1, ring, 0)
+    lax.fori_loop(s1 + 1, count + 1, spread, 0)
 
     for pos in range(4, 8):
         wv_copies[pos].wait()

time: 71.2 us -> 68.1 us (0.956)
  the two profiles are of different devices: /device:TPU:417 before, /device:TPU:33 now
where the time goes in v8:
time: 68.1 us; the launch traced here: 67.4 us
  Pallas kernels  65.1 us (96%)
  local copies, waits for them, and re-layouts  2.3 us (3%)
    pallas_call x1, Pallas kernels, body(): pl.pallas_call(kernel, out_shape=jax.ShapeDtypeStruct((mine, width), BF16...  65.1 us
    unnamed x1, local copies, waits for them, and re-layouts  2.3 us

profile of v8, /device:TPU:33, one launch (start us, length us, event | category | flops | bytes accessed | tf_op | source)
XLA Modules:
  0.0 67.4 jit_solution(13377122532112031976)
XLA Ops:
  0.0 65.1 %gated_recurrence.1 = bf16[256,2048]{1,0:T(8,128)(2,1)} custom-call(bf16[2048,2048]{1,0:T(8,128)(2,1)} %tokens_in.1, f32[16,128]{1,0:T(8,128)} %bitcast.8, bf16[2048,256]{1,0:T(8,128)(2,1)} %w_input_in.1, bf16[2048,256]{1,0:T(8,128)(2,1)} %w_gate_in.1, f32[4,256]{1,0:T(4,128)} %taps_in.1, bf16[256,256]{1,0:T(8,128)(2,1)} %bitcast.6, ...), custom_call_target="tpu_custom_call" | custom-call | tf_op jit(solution)/shard_map/gated_recurrence/pallas_call | solution.py:619
  65.1 2.3 %copy.13 = bf16[256,2048]{1,0:T(8,128)(2,1)} copy(bf16[256,2048]{1,0:T(8,128)(2,1)} %gated_recurrence.1) | data formatting | bytes 2097152

commit v9 on v8

--- a/solution.py
+++ b/solution.py
@@ -416,6 +416,8 @@
     lax.fori_loop(1, s0 + 1, spread, 0)
 
     r4 = goal(8, 5, 2, 5)
+    sooner = jnp.minimum(jnp.maximum(z - 1, 1), 8)
+    r4 = jnp.where(z > 0, (1 - core) * sooner + core * r4, r4)
     lax.fori_loop(r3 + 1, r4 + 1, ring, 0)
     s1 = goal(7, 4, 0, 2)
     lax.fori_loop(s0 + 1, s1 + 1, spread, 0)

time: 68.1 us -> 67.5 us (level)
  no operation moved by 1% of the time
where the time goes in v9:
time: 67.5 us; the launch traced here: 67.4 us
  Pallas kernels  65.1 us (96%)
  local copies, waits for them, and re-layouts  2.3 us (3%)
    pallas_call x1, Pallas kernels, body(): pl.pallas_call(kernel, out_shape=jax.ShapeDtypeStruct((mine, width), BF16...  65.1 us
    unnamed x1, local copies, waits for them, and re-layouts  2.3 us

profile of v9, /device:TPU:33, one launch (start us, length us, event | category | flops | bytes accessed | tf_op | source)
XLA Modules:
  0.0 67.4 jit_solution(4501013737827154334)
XLA Ops:
  0.0 65.1 %gated_recurrence.1 = bf16[256,2048]{1,0:T(8,128)(2,1)} custom-call(bf16[2048,2048]{1,0:T(8,128)(2,1)} %tokens_in.1, f32[16,128]{1,0:T(8,128)} %bitcast.8, bf16[2048,256]{1,0:T(8,128)(2,1)} %w_input_in.1, bf16[2048,256]{1,0:T(8,128)(2,1)} %w_gate_in.1, f32[4,256]{1,0:T(4,128)} %taps_in.1, bf16[256,256]{1,0:T(8,128)(2,1)} %bitcast.6, ...), custom_call_target="tpu_custom_call" | custom-call | tf_op jit(solution)/shard_map/gated_recurrence/pallas_call | solution.py:621
  65.1 2.3 %copy.13 = bf16[256,2048]{1,0:T(8,128)(2,1)} copy(bf16[256,2048]{1,0:T(8,128)(2,1)} %gated_recurrence.1) | data formatting | bytes 2097152
